TPU v7x, 32 devices: a whole 2x2x4 slice. The times are simulated.
32 devices in a mesh: rep: 4 (over z), fs: 4 (over y, x), tp: 2 (over core).
Axes of the slice: x: 2, y: 2, z: 4, core: 2. Of those that a mesh axis runs over, the one named last changes fastest.
Arguments:
- hidden_pre: bfloat16 [8192, 4096], P(('rep', 'fs'), 'tp'), may hold values from -6 to 6
- out_grad: bfloat16 [8192, 2048], P(('rep', 'fs')), may hold values from -8 to 8
- down_weight: bfloat16 [2048, 4096], P('fs', 'tp'), may hold values from -0.09375 to 0.09375
Outputs:
- hidden_grad: bfloat16 [8192, 4096], P(('rep', 'fs'), 'tp')
- weight_grad: float32 [2048, 4096], P('fs', 'tp')
All inputs are finite; a program needn't handle non-finite values.
Results may differ from a plain program's by a relative error of at most 0.0049.
Values may be sent and summed in bfloat16 or wider, within the bound.
A program may use at most 64 MiB of HBM per device.

v0:
```python
import math

import jax
import jax.numpy as jnp
from jax import lax
from jax.experimental import pallas as pl
from jax.experimental.pallas import tpu as pltpu
from jax.sharding import PartitionSpec as P

MESH = pl.DeviceIdType.MESH
BF = jnp.bfloat16
F32 = jnp.float32


def plain_body(hidden_pre, out_grad, down_weight):
    rows = hidden_pre.shape[0]
    ff_local = hidden_pre.shape[1]
    back = jnp.dot(
        out_grad,
        lax.all_gather(down_weight, "fs", axis=0, tiled=True),
        preferred_element_type=F32,
    )
    positive = jnp.maximum(hidden_pre.astype(F32), 0.0)
    hidden_grad = (2.0 * positive * back).astype(BF)
    act = (positive * positive).astype(BF)
    partial_value = lax.dot_general(
        out_grad, act, (((0,), (0,)), ((), ())), preferred_element_type=F32
    )
    partial_value = partial_value.astype(BF)
    received = lax.all_to_all(partial_value, "fs", split_axis=0, concat_axis=0, tiled=True)
    groups = lax.axis_size("fs")
    local_sum = jnp.sum(
        received.reshape(groups, received.shape[0] // groups, ff_local), axis=0, dtype=F32
    )
    total = lax.psum(local_sum, "rep")
    tokens_all = rows * lax.axis_size("rep") * groups
    return (hidden_grad, total * (1.0 / math.sqrt(tokens_all)))


STEPS = 4


def kernel(hp, og, w, hg_out, tot_out,
           ogcat, ogt, whalf, hpc, pbs, pbr, pbo, gs, gr, gown, zs, z1r, z2r, zt, hg,
           l_og, l_w, l_hp, o_hg, o_t,
           og_s, og_r, od_s, od_r, w_s, w_r, f_s, f_r, hp_s, hp_r, pb_s, pb_r, g_s, g_r,
           z1_s, z1_rs, z2_s, z2_rs, z3_s, z3_rs):
    rows, ff = hp.shape
    depth = w.shape[0]
    chunks = 2 * STEPS
    fc = ff // chunks
    part = rows // 2
    fs = lax.axis_index("fs")
    core = lax.axis_index("tp")
    z = lax.axis_index("rep")
    last = lax.axis_size("rep") - 1
    a, b = fs // 2, fs % 2
    par = z % 2
    apeer = {"fs": (1 - a) * 2 + b}
    bpeer = {"fs": a * 2 + (1 - b)}
    cpeer = {"tp": 1 - core}
    znext = {"rep": z + 1 - 2 * par}
    zmid = {"rep": last - z}
    outer = jnp.logical_or(z == 0, z == last)
    inner = jnp.logical_not(outer)
    token_peer = (apeer, bpeer)
    weight_peer = (bpeer, apeer)

    def remote(src, dst, ssem, rsem, peer):
        return pltpu.make_async_remote_copy(
            src_ref=src, dst_ref=dst, send_sem=ssem, recv_sem=rsem,
            device_id=peer, device_id_type=MESH)

    def cut(i, size):
        return pl.ds(pl.multiple_of(i * size, size), size)

    place = (b, a)
    mine = [cut(place[q], depth) for q in range(2)]
    theirs = [cut(1 - place[q], depth) for q in range(2)]
    own_block = lambda q, p: 2 * a + p if q == 0 else 2 * p + b
    far_block = lambda q, p: 2 * (1 - a) + p if q == 0 else 2 * p + 1 - b
    low = cut(core, part)
    mid = pl.ds(pl.multiple_of(rows + core * part, part), part)
    mid_other = pl.ds(pl.multiple_of(rows + (1 - core) * part, part), part)
    both = [(q, p) for q in range(2) for p in range(2)]

    def load_og(q, p):
        return pltpu.make_async_copy(
            og.at[:, cut(own_block(q, p), depth)],
            ogcat.at[q, pl.ds(0, rows), pl.ds(p * depth, depth)], l_og.at[q, p])

    def load_w(c, q):
        return pltpu.make_async_copy(w.at[:, cut(c, fc)], whalf.at[c, mine[q]], l_w.at[c])

    def load_hp(c):
        return pltpu.make_async_copy(hp.at[:, cut(c, fc)], hpc.at[0, c], l_hp.at[c])

    def store_hg(c):
        return pltpu.make_async_copy(hg.at[c], hg_out.at[:, cut(c, fc)], o_hg.at[c])

    def store_tot(c):
        return pltpu.make_async_copy(zt.at[c], tot_out.at[:, cut(c, fc)], o_t.at[c])

    def send_og(q, p):
        return remote(og.at[low, cut(far_block(q, p), depth)],
                      ogcat.at[q, mid, pl.ds(p * depth, depth)],
                      og_s.at[q, p], og_r.at[q, p], token_peer[q])

    def pass_og(q, p, span):
        spot = ogcat.at[q, span, pl.ds(p * depth, depth)]
        return remote(spot, spot, od_s.at[q, p], od_r.at[q, p], cpeer)

    def send_w(c, q):
        return remote(w.at[:, cut(c, fc)], whalf.at[c, mine[q]], w_s.at[c], w_r.at[c], weight_peer[q])

    def recv_w(c, q):
        return remote(w.at[:, cut(c, fc)], whalf.at[c, theirs[q]], w_s.at[c], w_r.at[c], weight_peer[q])

    def pass_w(c, q):
        spot = whalf.at[c, theirs[q]]
        return remote(spot, spot, f_s.at[c], f_r.at[c], znext)

    def send_hp(c, q):
        return remote(hp.at[:, cut(c, fc)], hpc.at[1, c], hp_s.at[c], hp_r.at[c], token_peer[q])

    def send_pb(c, q):
        return remote(pbs.at[c], pbr.at[c], pb_s.at[c], pb_r.at[c], token_peer[q])

    def send_g(c, q):
        return remote(gs.at[c], gr.at[c], g_s.at[c], g_r.at[c], weight_peer[q])

    def send_z1(c):
        return remote(zs.at[c], z1r.at[c], z1_s.at[c], z1_rs.at[c], znext)

    def send_z2(c):
        return remote(zs.at[c], z2r.at[c], z2_s.at[c], z2_rs.at[c], zmid)

    def send_z3(c):
        return remote(zt.at[c], zt.at[c], z3_s.at[c], z3_rs.at[c], znext)

    def kept(j, q):
        return 2 * (2 * j + par) + q

    def passed(j, q):
        return 2 * (2 * j + 1 - par) + q

    def g_step(s):
        for q in range(2):
            c = 2 * s + q
            load_hp(c).wait()
            send_hp(c, q).wait_recv()
            if s + 2 < STEPS:
                send_hp(c + 4, q).start()
            positive = jnp.maximum(hpc[:, c].reshape(2 * rows, fc).astype(F32), 0.0)
            act = (positive * positive).astype(BF)
            gs[c] = jnp.dot(ogt[q, theirs[q], :], act, preferred_element_type=F32).astype(BF)
            send_g(c, q).start()
            gown[c] = jnp.dot(ogt[q, mine[q], :], act, preferred_element_type=F32)

    def z_a(s):
        for q in range(2):
            c = 2 * s + q
            send_g(c, q).wait_recv()

            @pl.when(outer)
            def _():
                zs[c] = (gown[c] + gr[c].astype(F32)).astype(BF)
                send_z1(c).start()

    def z_b(s):
        @pl.when(inner)
        def _():
            for q in range(2):
                c = 2 * s + q
                send_z1(c).wait_recv()
                zs[c] = (gown[c] + gr[c].astype(F32) + z1r[c].astype(F32)).astype(BF)
                send_z2(c).start()

    def z_c(s):
        @pl.when(inner)
        def _():
            for q in range(2):
                c = 2 * s + q
                send_z2(c).wait_recv()
                zt[c] = (zs[c].astype(F32) + z2r[c].astype(F32)).astype(BF)
                send_z3(c).start()
                store_tot(c).start()

    def z_d(s):
        @pl.when(outer)
        def _():
            for q in range(2):
                c = 2 * s + q
                send_z3(c).wait_recv()
                store_tot(c).start()

    def back(c, q):
        load_w(c, q).wait()
        pbs[c] = jnp.dot(ogcat[q, rows:2 * rows, :], whalf[c], preferred_element_type=F32).astype(BF)
        send_pb(c, q).start()
        pbo[c] = jnp.dot(ogcat[q, 0:rows, :], whalf[c], preferred_element_type=F32)

    def pb_direct(j):
        for which in (kept, passed):
            for q in range(2):
                recv_w(which(j, q), q).wait_recv()
                back(which(j, q), q)

    def pb_first():
        for q in range(2):
            back(kept(0, q), q)
        for q in range(2):
            pass_w(passed(0, q), q).wait_recv()
            back(passed(0, q), q)

    def finish(which, j):
        for q in range(2):
            c = which(j, q)
            send_pb(c, q).wait_recv()
            positive = jnp.maximum(hpc[0, c].astype(F32), 0.0)
            hg[c] = (2.0 * positive * (pbo[c] + pbr[c].astype(F32))).astype(BF)
            store_hg(c).start()

    barrier = pltpu.get_barrier_semaphore()
    for peer in (apeer, bpeer, cpeer, znext, zmid):
        pl.semaphore_signal(barrier, inc=1, device_id=peer, device_id_type=MESH)
    for q, p in both:
        load_og(q, p).start()
    pl.semaphore_wait(barrier, 5)
    for q, p in both:
        send_og(q, p).start()
    for q in range(2):
        send_w(kept(0, q), q).start()
    for s in range(2):
        for q in range(2):
            send_hp(2 * s + q, q).start()
    for c in range(chunks):
        load_hp(c).start()
    for c in range(chunks):
        load_w(c, c % 2).start()
    for q, p in both:
        load_og(q, p).wait()
    for q in range(2):
        ogt[q, :, 0:rows] = ogcat[q, 0:rows, :].T
    for p in range(2):
        for q in range(2):
            send_og(q, p).wait_recv()
            pass_og(q, p, mid).start()
    for q in range(2):
        for p in range(2):
            pass_og(q, p, mid_other).wait_recv()
        ogt[q, :, rows:2 * rows] = ogcat[q, rows:2 * rows, :].T

    for q in range(2):
        recv_w(kept(0, q), q).wait_recv()
        pass_w(kept(0, q), q).start()

    g_step(0)
    g_step(1)
    z_a(0)
    g_step(2)
    z_a(1)
    g_step(3)
    z_b(0)
    pb_first()
    z_a(2)
    for which in (kept, passed):
        for q in range(2):
            send_w(which(1, q), q).start()
    z_a(3)
    z_b(1)
    z_c(0)
    z_b(2)
    z_c(1)
    pb_direct(1)
    z_b(3)
    finish(kept, 0)
    finish(passed, 0)
    z_c(2)
    z_c(3)
    finish(kept, 1)
    z_d(0)
    z_d(1)
    z_d(2)
    z_d(3)
    finish(passed, 1)

    for q, p in both:
        send_og(q, p).wait_send()
        pass_og(q, p, mid).wait_send()
    for q in range(2):
        pass_w(kept(0, q), q).wait_send()
        for c in (kept(0, q), kept(1, q), passed(1, q)):
            send_w(c, q).wait_send()
    for c in range(chunks):
        send_hp(c, c % 2).wait_send()
        send_pb(c, c % 2).wait_send()
        send_g(c, c % 2).wait_send()
        store_hg(c).wait()
        store_tot(c).wait()

    @pl.when(outer)
    def _():
        for c in range(chunks):
            send_z1(c).wait_send()

    @pl.when(inner)
    def _():
        for c in range(chunks):
            send_z2(c).wait_send()
            send_z3(c).wait_send()


def paired_body(hidden_pre, out_grad, down_weight):
    rows, ff = hidden_pre.shape
    depth = down_weight.shape[0]
    chunks = 2 * STEPS
    fc = ff // chunks
    any_spec = pl.BlockSpec(memory_space=pl.ANY)

    def block(r, dtype):
        return pltpu.VMEM((chunks, r, fc), dtype)

    sem = pltpu.SemaphoreType.DMA
    hidden_grad, total = pl.pallas_call(
        kernel,
        out_shape=(jax.ShapeDtypeStruct((rows, ff), BF), jax.ShapeDtypeStruct((depth, ff), BF)),
        in_specs=[any_spec] * 3,
        out_specs=(any_spec, any_spec),
        scratch_shapes=[
            pltpu.VMEM((2, 2 * rows, 2 * depth), BF),
            pltpu.VMEM((2, 2 * depth, 2 * rows), BF),
            block(2 * depth, BF),
            pltpu.VMEM((2, chunks, rows, fc), BF),
            block(rows, BF), block(rows, BF), block(rows, F32),
            block(depth, BF), block(depth, BF), block(depth, F32),
            block(depth, BF), block(depth, BF), block(depth, BF), block(depth, BF),
            block(rows, BF),
            sem((2, 2)), sem((chunks,)), sem((chunks,)), sem((chunks,)), sem((chunks,)),
        ] + [sem((2, 2))] * 4 + [sem((chunks,))] * 16,
        compiler_params=pltpu.CompilerParams(
            collective_id=0, has_side_effects=True, vmem_limit_bytes=60 * 1024 * 1024
        ),
    )(hidden_pre, out_grad, down_weight)
    tokens_all = rows * lax.axis_size("rep") * lax.axis_size("fs")
    return hidden_grad, total.astype(F32) * (1.0 / math.sqrt(tokens_all))


def solution(mesh):
    placed = (P(("rep", "fs"), "tp"), P(("rep", "fs"), None), P("fs", "tp"))
    two_by_two = mesh.shape["fs"] == 4 and mesh.shape["tp"] == 2 and mesh.shape["rep"] == 4
    return jax.shard_map(
        paired_body if two_by_two else plain_body,
        mesh=mesh,
        in_specs=placed,
        out_specs=(P(("rep", "fs"), "tp"), P("fs", "tp")),
        check_vma=False,
    )
```

profile of v0, /device:TPU:0, one launch (start us, length us, event | category | flops | bytes accessed | tf_op | source)
XLA Modules:
  0.0 125.7 jit_solution(3548139909442299896)
XLA Ops:
  0.6 119.4 %shard_map.50 = (bf16[512,2048]{1,0:T(8,128)(2,1)}, bf16[512,2048]{1,0:T(8,128)(2,1)}) custom-call(bf16[512,2048]{1,0:T(8,128)(2,1)} %hp.1, bf16[512,2048]{1,0:T(8,128)(2,1)} %og.1, bf16[512,2048]{1,0:T(8,128)(2,1)} %w.1), custom_call_target="tpu_custom_call" | custom-call | tf_op jit(solution)/shard_map/pallas_call | solution.py:325
  120.0 0.0 copy-start
  120.1 4.3 %convert_multiply_fusion = f32[512,2048]{1,0:T(8,128)} fusion(bf16[512,2048]{1,0:T(8,128)(2,1)} %get-tuple-element.5), kind=kLoop, calls=%fused_computation | loop fusion | flops 2097152 | bytes 6291456 | tf_op jit(solution)/shard_map/mul | solution.py:346
  124.4 0.0 copy-done
  124.4 1.3 %copy.6 = bf16[512,2048]{1,0:T(8,128)(2,1)} copy(bf16[512,2048]{1,0:T(8,128)(2,1)S(1)} %copy-done) | data formatting | bytes 4194304
Async XLA Ops:
  120.0 4.3 %copy-start = (bf16[512,2048]{1,0:T(8,128)(2,1)S(1)}, bf16[512,2048]{1,0:T(8,128)(2,1)}, u32[]{:S(2)}) copy-start(bf16[512,2048]{1,0:T(8,128)(2,1)} %get-tuple-element.8) | copy-start | bytes 6291460
where the time goes:
time: 126 us
  Pallas kernels  119 us (94%)
  other arithmetic  4.32 us (3%)
  local copies, waits for them, and re-layouts  1.32 us (1%)
    pallas_call x1, Pallas kernels, paired_body(): pl.pallas_call(kernel, out_shape=(jax.ShapeDtypeStruct((rows, ff), BF), j...  119 us
    mul x1, other arithmetic, paired_body(): return (hidden_grad, total.astype(F32) * (1.0 / math.sqrt(tokens_all)))  4.32 us

commit v1 on v0

v1 whole, which is shorter than its diff:
```python
import math

import jax
import jax.numpy as jnp
from jax import lax
from jax.experimental import pallas as pl
from jax.experimental.pallas import tpu as pltpu
from jax.sharding import PartitionSpec as P

MESH = pl.DeviceIdType.MESH
BF = jnp.bfloat16
F32 = jnp.float32


def plain_body(hidden_pre, out_grad, down_weight):
    rows = hidden_pre.shape[0]
    ff_local = hidden_pre.shape[1]
    back = jnp.dot(
        out_grad,
        lax.all_gather(down_weight, "fs", axis=0, tiled=True),
        preferred_element_type=F32,
    )
    positive = jnp.maximum(hidden_pre.astype(F32), 0.0)
    hidden_grad = (2.0 * positive * back).astype(BF)
    act = (positive * positive).astype(BF)
    partial_value = lax.dot_general(
        out_grad, act, (((0,), (0,)), ((), ())), preferred_element_type=F32
    )
    partial_value = partial_value.astype(BF)
    received = lax.all_to_all(partial_value, "fs", split_axis=0, concat_axis=0, tiled=True)
    groups = lax.axis_size("fs")
    local_sum = jnp.sum(
        received.reshape(groups, received.shape[0] // groups, ff_local), axis=0, dtype=F32
    )
    total = lax.psum(local_sum, "rep")
    tokens_all = rows * lax.axis_size("rep") * groups
    return (hidden_grad, total * (1.0 / math.sqrt(tokens_all)))


STEPS = 4
PIECES = ((0, 0, 1), (0, 1, 1), (1, 0, 2), (2, 0, 2), (3, 0, 2))


def kernel(hp, og, w, hg_out, tot_out,
           ogcat, ogt, whalf, hpc, pbs, pbr, pbo, gs, gr, gown, zs, z1r, z2r, zt,
           l_og, l_w, l_hp,
           og_s, og_r, od_s, od_r, w_s, w_r, fn_s, fm_s, f_r, pb_s, pb_r,
           hp_s, hp_r, g_s, g_r, z1_s, z1_rs, z2_s, z2_rs, z3_s, z3_rs):
    rows, ff = hp.shape
    depth = w.shape[0]
    half = ff // 2
    fc = half // STEPS
    unit = fc // 2
    part = rows // 2
    piece_rows = depth // 2
    fs = lax.axis_index("fs")
    core = lax.axis_index("tp")
    z = lax.axis_index("rep")
    last = lax.axis_size("rep") - 1
    a, b = fs // 2, fs % 2
    znear = z + 1 - 2 * (z % 2)
    apeer = {"fs": (1 - a) * 2 + b}
    bpeer = {"fs": a * 2 + (1 - b)}
    cpeer = {"tp": 1 - core}
    znext = {"rep": znear}
    zmid = {"rep": last - z}
    outer = jnp.logical_or(z == 0, z == last)
    inner = jnp.logical_not(outer)
    token_peer = (apeer, bpeer)
    weight_peer = (bpeer, apeer)
    scale = 1.0 / math.sqrt(rows * lax.axis_size("rep") * lax.axis_size("fs"))
    count = len(PIECES)

    def remote(src, dst, ssem, rsem, peer):
        return pltpu.make_async_remote_copy(
            src_ref=src, dst_ref=dst, send_sem=ssem, recv_sem=rsem,
            device_id=peer, device_id_type=MESH)

    def cut(i, size):
        return pl.ds(pl.multiple_of(i * size, size), size)

    place = (b, a)
    mine = [cut(place[q], depth) for q in range(2)]
    theirs = [cut(1 - place[q], depth) for q in range(2)]
    far_block = lambda q, p: 2 * (1 - a) + p if q == 0 else 2 * p + 1 - b
    own_block = lambda q, p: 2 * a + p if q == 0 else 2 * p + b
    low = cut(core, part)
    mid = pl.ds(pl.multiple_of(rows + core * part, part), part)
    mid_other = pl.ds(pl.multiple_of(rows + (1 - core) * part, part), part)
    both = [(q, p) for q in range(2) for p in range(2)]
    halves = range(2)

    def their_rows(q, h):
        return cut(2 * (1 - place[q]) + h, piece_rows)

    def piece_cols(k):
        j, first, units = PIECES[k]
        return j, pl.ds(first * unit, units * unit)

    def hp_cols(q, k):
        j, first, units = PIECES[k]
        return pl.ds(q * half + j * fc + first * unit, units * unit)

    def chunk(q, j):
        return q * STEPS + j

    def load_og(q, p):
        return pltpu.make_async_copy(
            og.at[:, cut(own_block(q, p), depth)],
            ogcat.at[q, pl.ds(0, rows), pl.ds(p * depth, depth)], l_og.at[q, p])

    def load_w(c):
        return pltpu.make_async_copy(
            w.at[:, pl.ds(c * fc, fc)], whalf.at[c, mine[c // STEPS]], l_w.at[c])

    def load_hp(c):
        return pltpu.make_async_copy(hp.at[:, pl.ds(c * fc, fc)], hpc.at[0, c], l_hp.at[c])

    def send_og(q, p):
        return remote(og.at[low, cut(far_block(q, p), depth)],
                      ogcat.at[q, mid, cut(p, depth)],
                      og_s.at[q, p], og_r.at[q, p], token_peer[q])

    def pass_og(q, p, span):
        spot = ogcat.at[q, span, cut(p, depth)]
        return remote(spot, spot, od_s.at[q, p], od_r.at[q, p], cpeer)

    def send_w(q):
        return remote(w.at[:, cut(chunk(q, z), fc)], whalf.at[chunk(q, z), mine[q]],
                      w_s.at[q], w_r.at[q], weight_peer[q])

    def pass_w(q, j, peer, ssem):
        spot = whalf.at[chunk(q, j), theirs[q]]
        return remote(spot, spot, ssem.at[chunk(q, j)], f_r.at[chunk(q, j)], peer)

    def near_w(q, j):
        return pass_w(q, j, znext, fn_s)

    def mid_w(q, j):
        return pass_w(q, j, zmid, fm_s)

    def send_hp(q, k):
        j, cols = piece_cols(k)
        return remote(hp.at[:, hp_cols(q, k)], hpc.at[1, chunk(q, j), :, cols],
                      hp_s.at[q, k], hp_r.at[q, k], token_peer[q])

    def send_pb(q, j):
        c = chunk(q, j)
        return remote(pbs.at[c], pbr.at[c], pb_s.at[c], pb_r.at[c], token_peer[q])

    def strip(ref, q, k, h):
        j, cols = piece_cols(k)
        return ref.at[chunk(q, j), pl.ds(h * piece_rows, piece_rows), cols]

    def send_g(q, k, h):
        return remote(strip(gs, q, k, h), strip(gr, q, k, h),
                      g_s.at[q, k, h], g_r.at[q, k, h], weight_peer[q])

    def send_z1(q, k, h):
        return remote(strip(zs, q, k, h), strip(z1r, q, k, h),
                      z1_s.at[q, k, h], z1_rs.at[q, k, h], znext)

    def send_z2(q, k, h):
        return remote(strip(zs, q, k, h), strip(z2r, q, k, h),
                      z2_s.at[q, k, h], z2_rs.at[q, k, h], zmid)

    def send_z3(q, k, h):
        return remote(strip(zt, q, k, h), strip(zt, q, k, h),
                      z3_s.at[q, k, h], z3_rs.at[q, k, h], znext)

    def act_of(q, k):
        j, cols = piece_cols(k)
        held = hpc[:, chunk(q, j), :, cols]
        positive = jnp.maximum(held.reshape(2 * rows, held.shape[-1]).astype(F32), 0.0)
        return (positive * positive).astype(BF)

    def g_out(q, k, act):
        for h in halves:
            strip(gs, q, k, h)[...] = jnp.dot(
                ogt[q, their_rows(q, h), :], act, preferred_element_type=F32).astype(BF)
            send_g(q, k, h).start()

    def g_own(q, k, act):
        j, cols = piece_cols(k)
        gown[chunk(q, j), :, cols] = jnp.dot(
            ogt[q, mine[q], :], act, preferred_element_type=F32)

    def got_hp(q, k):
        if PIECES[k][1] == 0:
            load_hp(chunk(q, PIECES[k][0])).wait()
        send_hp(q, k).wait_recv()

    def g_step(k, then):
        for q in range(2):
            got_hp(q, k)
            act = act_of(q, k)
            g_out(q, k, act)
            for n in then:
                send_hp(q, n).start()
            g_own(q, k, act)

    def each(k):
        return [(q, h) for q in range(2) for h in halves]

    def z_a(k):
        for q, h in each(k):
            send_g(q, k, h).wait_recv()

            @pl.when(outer)
            def _():
                strip(zs, q, k, h)[...] = (
                    strip(gown, q, k, h)[...] + strip(gr, q, k, h)[...].astype(F32)).astype(BF)
                send_z1(q, k, h).start()

    def z_b(k):
        @pl.when(inner)
        def _():
            for q, h in each(k):
                send_z1(q, k, h).wait_recv()
                strip(zs, q, k, h)[...] = (
                    strip(gown, q, k, h)[...] + strip(gr, q, k, h)[...].astype(F32)
                    + strip(z1r, q, k, h)[...].astype(F32)).astype(BF)
                send_z2(q, k, h).start()

    def put_total(q, k, h, value):
        j, first, units = PIECES[k]
        tot_out[h * piece_rows:(h + 1) * piece_rows,
                q * half + j * fc + first * unit:q * half + j * fc + (first + units) * unit
                ] = value

    def z_c(k):
        @pl.when(inner)
        def _():
            for q, h in each(k):
                send_z2(q, k, h).wait_recv()
                value = (strip(zs, q, k, h)[...].astype(F32)
                         + strip(z2r, q, k, h)[...].astype(F32)).astype(BF)
                strip(zt, q, k, h)[...] = value
                send_z3(q, k, h).start()
                put_total(q, k, h, value)

    def z_d(k):
        @pl.when(outer)
        def _():
            for q, h in each(k):
                send_z3(q, k, h).wait_recv()
                put_total(q, k, h, strip(zt, q, k, h)[...])

    order = (z, znear, jnp.where(outer, last - znear, last - z), jnp.where(outer, last - z, last - znear))

    def w_first():
        for q in range(2):
            send_w(q).wait_recv()
            near_w(q, z).start()

            @pl.when(inner)
            def _():
                mid_w(q, z).start()

    def w_second():
        for q in range(2):
            @pl.when(inner)
            def _():
                mid_w(q, last - z).wait_recv()
                near_w(q, last - z).start()
                near_w(q, znear).wait_recv()
                mid_w(q, znear).start()

    def w_third():
        for q in range(2):
            @pl.when(inner)
            def _():
                mid_w(q, last - znear).wait_recv()
                near_w(q, last - znear).start()

    def got_w(q, i):
        if i == 1:
            @pl.when(outer)
            def _():
                near_w(q, order[1]).wait_recv()
        elif i > 1:
            @pl.when(outer)
            def _():
                near_w(q, order[i]).wait_recv()

    def back_one(q, i):
        c = chunk(q, order[i])
        got_w(q, i)
        pbs[c] = jnp.dot(ogcat[q, rows:2 * rows, :], whalf[c], preferred_element_type=F32).astype(BF)
        send_pb(q, order[i]).start()
        pbo[c] = jnp.dot(ogcat[q, 0:rows, :], whalf[c], preferred_element_type=F32)

    def back(i):
        for q in range(2):
            back_one(q, i)

    def finish(i):
        for q in range(2):
            c = chunk(q, order[i])
            send_pb(q, order[i]).wait_recv()
            positive = jnp.maximum(hpc[0, c].astype(F32), 0.0)
            hg_out[:, cut(c, fc)] = (2.0 * positive * (pbo[c] + pbr[c].astype(F32))).astype(BF)

    def og_arrive(far):
        for q in range(2):
            p = 1 - place[q] if far else place[q]
            send_og(q, p).wait_recv()
            pass_og(q, p, mid).start()
        for q in range(2):
            p = 1 - place[q] if far else place[q]
            pass_og(q, p, mid_other).wait_recv()
            ogt[q, cut(p, depth), rows:2 * rows] = ogcat[q, rows:2 * rows, cut(p, depth)].T

    barrier = pltpu.get_barrier_semaphore()
    for peer in (apeer, bpeer, cpeer, znext, zmid):
        pl.semaphore_signal(barrier, inc=1, device_id=peer, device_id_type=MESH)
    for q, p in both:
        load_og(q, p).start()
    pl.semaphore_wait(barrier, 5)
    for q in range(2):
        send_w(q).start()
    for q in range(2):
        send_og(q, 1 - place[q]).start()
    for q in range(2):
        send_hp(q, 0).start()
    for q in range(2):
        send_og(q, place[q]).start()
    for k in (1, 2):
        for q in range(2):
            send_hp(q, k).start()
    for c in range(2 * STEPS):
        load_hp(c).start()
    for c in range(2 * STEPS):
        load_w(c).start()
    for q, p in both:
        load_og(q, p).wait()
    for q in range(2):
        ogt[q, :, 0:rows] = ogcat[q, 0:rows, :].T
    w_first()
    og_arrive(True)
    for q in range(2):
        got_hp(q, 0)
        g_out(q, 0, act_of(q, 0))
    w_second()
    og_arrive(False)
    for q in range(2):
        g_own(q, 0, act_of(q, 0))
    for c in range(2 * STEPS):
        load_w(c).wait()
    g_step(1, (3,))
    w_third()
    z_a(0)
    g_step(2, (4,))
    z_b(0)
    z_a(1)
    z_b(1)
    g_step(3, ())
    z_c(0)
    z_a(2)
    z_c(1)
    z_b(2)
    g_step(4, ())
    back(0)
    z_c(2)
    z_a(3)
    z_b(3)
    back(1)
    z_a(4)
    z_c(3)
    z_b(4)
    back(2)
    back(3)
    finish(0)
    z_c(4)
    for k in range(count - 1):
        z_d(k)
    finish(1)
    finish(2)
    z_d(count - 1)
    finish(3)

    for q, p in both:
        send_og(q, p).wait_send()
        pass_og(q, p, mid).wait_send()
    for q in range(2):
        send_w(q).wait_send()
        near_w(q, z).wait_send()
        for k in range(count):
            send_hp(q, k).wait_send()
        for j in range(STEPS):
            send_pb(q, j).wait_send()
    pieces = [(q, k, h) for k in range(count) for q in range(2) for h in halves]
    for q, k, h in pieces:
        send_g(q, k, h).wait_send()

    @pl.when(outer)
    def _():
        for q, k, h in pieces:
            send_z1(q, k, h).wait_send()

    @pl.when(inner)
    def _():
        for q in range(2):
            mid_w(q, z).wait_send()
            mid_w(q, znear).wait_send()
            near_w(q, last - z).wait_send()
            near_w(q, last - znear).wait_send()
        for q, k, h in pieces:
            send_z2(q, k, h).wait_send()
            send_z3(q, k, h).wait_send()


def paired_body(hidden_pre, out_grad, down_weight):
    rows, ff = hidden_pre.shape
    depth = down_weight.shape[0]
    chunks = 2 * STEPS
    fc = ff // chunks
    count = len(PIECES)
    any_spec = pl.BlockSpec(memory_space=pl.ANY)
    vmem_spec = pl.BlockSpec(memory_space=pltpu.VMEM)

    def block(r, dtype):
        return pltpu.VMEM((chunks, r, fc), dtype)

    sem = pltpu.SemaphoreType.DMA
    hidden_grad, total = pl.pallas_call(
        kernel,
        out_shape=(jax.ShapeDtypeStruct((rows, ff), BF), jax.ShapeDtypeStruct((depth, ff), BF)),
        in_specs=[any_spec] * 3,
        out_specs=(vmem_spec, vmem_spec),
        scratch_shapes=[
            pltpu.VMEM((2, 2 * rows, 2 * depth), BF),
            pltpu.VMEM((2, 2 * depth, 2 * rows), BF),
            block(2 * depth, BF),
            pltpu.VMEM((2, chunks, rows, fc), BF),
            block(rows, BF), block(rows, BF), block(rows, F32),
            block(depth, BF), block(depth, BF), block(depth, F32),
            block(depth, BF), block(depth, BF), block(depth, BF), block(depth, BF),
            sem((2, 2)), sem((chunks,)), sem((chunks,)),
        ] + [sem((2, 2))] * 4 + [sem((2,))] * 2 + [sem((chunks,))] * 5
        + [sem((2, count))] * 2 + [sem((2, count, 2))] * 8,
        compiler_params=pltpu.CompilerParams(
            collective_id=0, has_side_effects=True, vmem_limit_bytes=48 * 1024 * 1024
        ),
    )(hidden_pre, out_grad, down_weight)
    tokens_all = rows * lax.axis_size("rep") * lax.axis_size("fs")
    return hidden_grad, total.astype(F32) * (1.0 / math.sqrt(tokens_all))


def solution(mesh):
    placed = (P(("rep", "fs"), "tp"), P(("rep", "fs"), None), P("fs", "tp"))
    two_by_two = mesh.shape["fs"] == 4 and mesh.shape["tp"] == 2 and mesh.shape["rep"] == 4
    return jax.shard_map(
        paired_body if two_by_two else plain_body,
        mesh=mesh,
        in_specs=placed,
        out_specs=(P(("rep", "fs"), "tp"), P("fs", "tp")),
        check_vma=False,
    )
```

time: 126 us -> 109 us (0.87)
  Pallas kernels: 119 us -> 105 us
  other arithmetic: 4.32 us -> 2.59 us
    pallas_call x1, Pallas kernels: 119 us -> 105 us  [paired_body(): pl.pallas_call(kernel, out_shape=(jax.ShapeDtypeStruct((rows, ff), BF), j...]
    mul x1, other arithmetic: 4.32 us -> 2.59 us  [paired_body(): return (hidden_grad, total.astype(F32) * (1.0 / math.sqrt(tokens_all)))]
where the time goes in v1:
time: 109 us
  Pallas kernels  105 us (96%)
  other arithmetic  2.59 us (2%)
  local copies, waits for them, and re-layouts  1.32 us (1%)
    pallas_call x1, Pallas kernels, paired_body(): pl.pallas_call(kernel, out_shape=(jax.ShapeDtypeStruct((rows, ff), BF), j...  105 us
    mul x1, other arithmetic, paired_body(): return (hidden_grad, total.astype(F32) * (1.0 / math.sqrt(tokens_all)))  2.59 us

profile of v1, /device:TPU:0, one launch (start us, length us, event | category | flops | bytes accessed | tf_op | source)
XLA Modules:
  0.0 109.0 jit_solution(3909118935716136097)
XLA Ops:
  0.6 104.5 %shard_map.50 = (bf16[512,2048]{1,0:T(8,128)(2,1)S(1)}, bf16[512,2048]{1,0:T(8,128)(2,1)S(1)}) custom-call(bf16[512,2048]{1,0:T(8,128)(2,1)} %hp.1, bf16[512,2048]{1,0:T(8,128)(2,1)} %og.1, bf16[512,2048]{1,0:T(8,128)(2,1)} %w.1), custom_call_target="tpu_custom_call" | custom-call | tf_op jit(solution)/shard_map/pallas_call | solution.py:426
  105.1 2.6 %convert_multiply_fusion = f32[512,2048]{1,0:T(8,128)} fusion(bf16[512,2048]{1,0:T(8,128)(2,1)S(1)} %get-tuple-element.5), kind=kLoop, calls=%fused_computation | loop fusion | flops 2097152 | bytes 6291456 | tf_op jit(solution)/shard_map/mul | solution.py:447
  107.7 1.3 %copy.6 = bf16[512,2048]{1,0:T(8,128)(2,1)} copy(bf16[512,2048]{1,0:T(8,128)(2,1)S(1)} %get-tuple-element.8) | data formatting | bytes 4194304

commit v2 on v1

--- a/solution.py
+++ b/solution.py
@@ -39,6 +39,39 @@
 
 STEPS = 4
 PIECES = ((0, 0, 1), (0, 1, 1), (1, 0, 2), (2, 0, 2), (3, 0, 2))
+PUTS = 4
+PARTS = 2
+WPARTS = 2
+PLAN = (
+    ("sw", 1, 0), ("sw", 0, 1), ("sw", 0, 0), ("sw", 1, 1), ("sog", 0, 1), ("sog", 0, 0), ("sog", 1, 1),
+    ("w1", 1, 0), ("tr0", 1), ("w1", 0, 0), ("shp", 0, 3), ("sog", 1, 0), ("w2b", 1, 0), ("w1", 1, 1),
+    ("shp", 0, 1), ("shp", 1, 1), ("w2a", 1, 0), ("w2b", 1, 1), ("w3", 1, 0), ("w1", 0, 1), ("w2a", 0, 0),
+    ("shp", 1, 2), ("ogr", 1, 1), ("ogr", 0, 1), ("tr0", 0), ("w2b", 0, 1), ("ogr", 1, 0), ("ogr", 0, 0),
+    ("w2a", 1, 1), ("ogt", 0, 1), ("ogt", 1, 1), ("shp", 0, 0), ("gout", 1, 1), ("ogt", 0, 0),
+    ("gout", 0, 3), ("shp", 0, 2), ("w3", 1, 1), ("w2a", 0, 1), ("w2b", 0, 0), ("gown", 0, 3),
+    ("gout", 1, 2), ("gout", 0, 1), ("shp", 0, 4), ("ogt", 1, 0), ("w3", 0, 0), ("za", 0, 3, 0),
+    ("gout", 0, 0), ("za", 0, 3, 1), ("w3", 0, 1), ("shp", 1, 0), ("shp", 1, 3), ("zb", 0, 3, 0),
+    ("zb", 0, 3, 1), ("gown", 0, 1), ("zc", 0, 3, 0), ("gown", 1, 1), ("za", 0, 1, 0), ("za", 0, 1, 1),
+    ("za", 1, 1, 0), ("za", 1, 1, 1), ("zb", 0, 1, 0), ("zb", 0, 1, 1), ("gown", 1, 2), ("gout", 0, 2),
+    ("zb", 1, 1, 1), ("shp", 1, 4), ("za", 1, 2, 0), ("za", 1, 2, 1), ("zb", 1, 1, 0), ("zc", 0, 3, 1),
+    ("gown", 0, 0), ("zb", 1, 2, 0), ("zc", 0, 1, 1), ("gown", 0, 2), ("gout", 1, 0), ("za", 0, 0, 0),
+    ("gout", 1, 3), ("za", 0, 0, 1), ("za", 0, 2, 0), ("zc", 1, 1, 1), ("bk", 0, 2), ("gown", 1, 0),
+    ("zc", 1, 1, 0), ("zd", 0, 1, 1), ("za", 1, 0, 1), ("zd", 1, 1, 0), ("zb", 1, 2, 1), ("zc", 0, 1, 0),
+    ("gown", 1, 3), ("za", 0, 2, 1), ("zc", 1, 2, 0), ("zb", 0, 0, 0), ("gout", 0, 4), ("zd", 0, 3, 1),
+    ("zb", 0, 0, 1), ("zc", 1, 2, 1), ("bk", 1, 0), ("zb", 0, 2, 0), ("zb", 1, 0, 1), ("za", 1, 3, 0),
+    ("zc", 0, 0, 1), ("bko", 0, 2), ("zc", 0, 0, 0), ("zb", 0, 2, 1), ("gout", 1, 4), ("za", 1, 3, 1),
+    ("za", 1, 0, 0), ("zc", 0, 2, 0), ("zb", 1, 3, 0), ("zc", 0, 2, 1), ("bko", 1, 0), ("gown", 0, 4),
+    ("gown", 1, 4), ("za", 0, 4, 1), ("za", 0, 4, 0), ("zd", 0, 2, 0), ("zb", 1, 3, 1), ("bk", 0, 1),
+    ("bk", 1, 1), ("zc", 1, 0, 1), ("bk", 1, 3), ("bk", 0, 0), ("zc", 1, 3, 0), ("bko", 0, 1),
+    ("zb", 0, 4, 1), ("za", 1, 4, 0), ("bko", 1, 1), ("zd", 0, 0, 1), ("za", 1, 4, 1), ("zc", 1, 3, 1),
+    ("zd", 1, 0, 1), ("zb", 0, 4, 0), ("zd", 1, 3, 1), ("bk", 1, 2), ("zc", 0, 4, 1), ("zb", 1, 4, 0),
+    ("zd", 0, 1, 0), ("bko", 1, 3), ("bk", 0, 3), ("fin", 1, 0), ("bko", 0, 3), ("zc", 0, 4, 0),
+    ("zd", 0, 3, 0), ("bko", 0, 0), ("zb", 1, 4, 1), ("fin", 1, 1), ("bko", 1, 2), ("zb", 1, 0, 0),
+    ("zc", 1, 4, 0), ("zd", 0, 0, 0), ("fin", 1, 3), ("zc", 1, 4, 1), ("zd", 0, 2, 1), ("fin", 0, 2),
+    ("fin", 0, 1), ("fin", 0, 0), ("zd", 1, 4, 1), ("zd", 1, 2, 1), ("zc", 1, 0, 0), ("zd", 1, 1, 1),
+    ("zd", 1, 3, 0), ("zd", 0, 4, 0), ("zd", 1, 4, 0), ("fin", 0, 3), ("zd", 1, 2, 0), ("fin", 1, 2),
+    ("zd", 0, 4, 1), ("zd", 1, 0, 0),
+)
 
 
 def kernel(hp, og, w, hg_out, tot_out,
@@ -52,7 +85,8 @@
     fc = half // STEPS
     unit = fc // 2
     part = rows // 2
-    piece_rows = depth // 2
+    w_rows = depth // WPARTS
+    piece_rows = depth // PARTS
     fs = lax.axis_index("fs")
     core = lax.axis_index("tp")
     z = lax.axis_index("rep")
@@ -88,10 +122,10 @@
     mid = pl.ds(pl.multiple_of(rows + core * part, part), part)
     mid_other = pl.ds(pl.multiple_of(rows + (1 - core) * part, part), part)
     both = [(q, p) for q in range(2) for p in range(2)]
-    halves = range(2)
+    halves = range(PARTS)
 
     def their_rows(q, h):
-        return cut(2 * (1 - place[q]) + h, piece_rows)
+        return cut(PARTS * (1 - place[q]) + h, piece_rows)
 
     def piece_cols(k):
         j, first, units = PIECES[k]
@@ -125,19 +159,22 @@
         spot = ogcat.at[q, span, cut(p, depth)]
         return remote(spot, spot, od_s.at[q, p], od_r.at[q, p], cpeer)
 
-    def send_w(q):
-        return remote(w.at[:, cut(chunk(q, z), fc)], whalf.at[chunk(q, z), mine[q]],
-                      w_s.at[q], w_r.at[q], weight_peer[q])
-
-    def pass_w(q, j, peer, ssem):
-        spot = whalf.at[chunk(q, j), theirs[q]]
-        return remote(spot, spot, ssem.at[chunk(q, j)], f_r.at[chunk(q, j)], peer)
-
-    def near_w(q, j):
-        return pass_w(q, j, znext, fn_s)
-
-    def mid_w(q, j):
-        return pass_w(q, j, zmid, fm_s)
+    def send_w(q, h):
+        c = chunk(q, z)
+        return remote(w.at[h * w_rows:(h + 1) * w_rows, cut(c, fc)],
+                      whalf.at[c, cut(WPARTS * place[q] + h, w_rows)],
+                      w_s.at[q, h], w_r.at[q, h], weight_peer[q])
+
+    def pass_w(q, j, h, peer, ssem):
+        c = chunk(q, j)
+        spot = whalf.at[c, cut(WPARTS * (1 - place[q]) + h, w_rows)]
+        return remote(spot, spot, ssem.at[c, h], f_r.at[c, h], peer)
+
+    def near_w(q, j, h):
+        return pass_w(q, j, h, znext, fn_s)
+
+    def mid_w(q, j, h):
+        return pass_w(q, j, h, zmid, fm_s)
 
     def send_hp(q, k):
         j, cols = piece_cols(k)
@@ -185,42 +222,53 @@
         gown[chunk(q, j), :, cols] = jnp.dot(
             ogt[q, mine[q], :], act, preferred_element_type=F32)
 
-    def got_hp(q, k):
-        if PIECES[k][1] == 0:
-            load_hp(chunk(q, PIECES[k][0])).wait()
+    loaded = set()
+
+    def once(name, copies):
+        if name not in loaded:
+            loaded.add(name)
+            for copy in copies():
+                copy.wait()
+
+    def transpose_own(q):
+        once("og", lambda: [load_og(*at) for at in both])
+        ogt[q, :, 0:rows] = ogcat[q, 0:rows, :].T
+
+    def og_part(q, far):
+        return 1 - place[q] if far else place[q]
+
+    def og_relay(q, far):
+        p = og_part(q, far)
+        send_og(q, p).wait_recv()
+        pass_og(q, p, mid).start()
+
+    def og_whole(q, far):
+        p = og_part(q, far)
+        pass_og(q, p, mid_other).wait_recv()
+        ogt[q, cut(p, depth), rows:2 * rows] = ogcat[q, rows:2 * rows, cut(p, depth)].T
+
+    def grad_send(q, k):
+        c = chunk(q, PIECES[k][0])
+        once(c, lambda: [load_hp(c)])
         send_hp(q, k).wait_recv()
-
-    def g_step(k, then):
-        for q in range(2):
-            got_hp(q, k)
-            act = act_of(q, k)
-            g_out(q, k, act)
-            for n in then:
-                send_hp(q, n).start()
-            g_own(q, k, act)
-
-    def each(k):
-        return [(q, h) for q in range(2) for h in halves]
-
-    def z_a(k):
-        for q, h in each(k):
-            send_g(q, k, h).wait_recv()
-
-            @pl.when(outer)
-            def _():
-                strip(zs, q, k, h)[...] = (
-                    strip(gown, q, k, h)[...] + strip(gr, q, k, h)[...].astype(F32)).astype(BF)
-                send_z1(q, k, h).start()
-
-    def z_b(k):
-        @pl.when(inner)
-        def _():
-            for q, h in each(k):
-                send_z1(q, k, h).wait_recv()
-                strip(zs, q, k, h)[...] = (
-                    strip(gown, q, k, h)[...] + strip(gr, q, k, h)[...].astype(F32)
-                    + strip(z1r, q, k, h)[...].astype(F32)).astype(BF)
-                send_z2(q, k, h).start()
+        g_out(q, k, act_of(q, k))
+
+    def grad_keep(q, k):
+        g_own(q, k, act_of(q, k))
+
+    def z_outer_send(q, k, h):
+        send_g(q, k, h).wait_recv()
+        strip(zs, q, k, h)[...] = (
+            strip(gown, q, k, h)[...] + strip(gr, q, k, h)[...].astype(F32)).astype(BF)
+        send_z1(q, k, h).start()
+
+    def z_inner_send(q, k, h):
+        send_g(q, k, h).wait_recv()
+        send_z1(q, k, h).wait_recv()
+        strip(zs, q, k, h)[...] = (
+            strip(gown, q, k, h)[...] + strip(gr, q, k, h)[...].astype(F32)
+            + strip(z1r, q, k, h)[...].astype(F32)).astype(BF)
+        send_z2(q, k, h).start()
 
     def put_total(q, k, h, value):
         j, first, units = PIECES[k]
@@ -228,88 +276,79 @@
                 q * half + j * fc + first * unit:q * half + j * fc + (first + units) * unit
                 ] = value
 
-    def z_c(k):
+    def z_inner_last(q, k, h):
+        send_z2(q, k, h).wait_recv()
+        value = (strip(zs, q, k, h)[...].astype(F32)
+                 + strip(z2r, q, k, h)[...].astype(F32)).astype(BF)
+        strip(zt, q, k, h)[...] = value
+        send_z3(q, k, h).start()
+        put_total(q, k, h, value)
+
+    def z_outer_last(q, k, h):
+        send_z3(q, k, h).wait_recv()
+        put_total(q, k, h, strip(zt, q, k, h)[...])
+
+    order = (z, znear, jnp.where(outer, last - znear, last - z), jnp.where(outer, last - z, last - znear))
+
+    def w_own(q, h):
+        send_w(q, h).wait_recv()
+        near_w(q, z, h).start()
+
         @pl.when(inner)
         def _():
-            for q, h in each(k):
-                send_z2(q, k, h).wait_recv()
-                value = (strip(zs, q, k, h)[...].astype(F32)
-                         + strip(z2r, q, k, h)[...].astype(F32)).astype(BF)
-                strip(zt, q, k, h)[...] = value
-                send_z3(q, k, h).start()
-                put_total(q, k, h, value)
-
-    def z_d(k):
-        @pl.when(outer)
-        def _():
-            for q, h in each(k):
-                send_z3(q, k, h).wait_recv()
-                put_total(q, k, h, strip(zt, q, k, h)[...])
-
-    order = (z, znear, jnp.where(outer, last - znear, last - z), jnp.where(outer, last - z, last - znear))
-
-    def w_first():
-        for q in range(2):
-            send_w(q).wait_recv()
-            near_w(q, z).start()
-
-            @pl.when(inner)
-            def _():
-                mid_w(q, z).start()
-
-    def w_second():
-        for q in range(2):
-            @pl.when(inner)
-            def _():
-                mid_w(q, last - z).wait_recv()
-                near_w(q, last - z).start()
-                near_w(q, znear).wait_recv()
-                mid_w(q, znear).start()
-
-    def w_third():
-        for q in range(2):
-            @pl.when(inner)
-            def _():
-                mid_w(q, last - znear).wait_recv()
-                near_w(q, last - znear).start()
-
-    def got_w(q, i):
-        if i == 1:
+            mid_w(q, z, h).start()
+
+    def w_down(q, h):
+        mid_w(q, last - z, h).wait_recv()
+        near_w(q, last - z, h).start()
+
+    def w_across(q, h):
+        near_w(q, znear, h).wait_recv()
+        mid_w(q, znear, h).start()
+
+    def w_far(q, h):
+        mid_w(q, last - znear, h).wait_recv()
+        near_w(q, last - znear, h).start()
+
+    def back_send(q, i):
+        once("w", lambda: [load_w(c) for c in range(2 * STEPS)])
+        c = chunk(q, order[i])
+        if i > 0:
             @pl.when(outer)
             def _():
-                near_w(q, order[1]).wait_recv()
-        elif i > 1:
-            @pl.when(outer)
-            def _():
-                near_w(q, order[i]).wait_recv()
-
-    def back_one(q, i):
-        c = chunk(q, order[i])
-        got_w(q, i)
+                for h in range(WPARTS):
+                    near_w(q, order[i], h).wait_recv()
         pbs[c] = jnp.dot(ogcat[q, rows:2 * rows, :], whalf[c], preferred_element_type=F32).astype(BF)
         send_pb(q, order[i]).start()
+
+    def back_keep(q, i):
+        c = chunk(q, order[i])
         pbo[c] = jnp.dot(ogcat[q, 0:rows, :], whalf[c], preferred_element_type=F32)
 
-    def back(i):
-        for q in range(2):
-            back_one(q, i)
-
-    def finish(i):
-        for q in range(2):
-            c = chunk(q, order[i])
-            send_pb(q, order[i]).wait_recv()
-            positive = jnp.maximum(hpc[0, c].astype(F32), 0.0)
-            hg_out[:, cut(c, fc)] = (2.0 * positive * (pbo[c] + pbr[c].astype(F32))).astype(BF)
-
-    def og_arrive(far):
-        for q in range(2):
-            p = 1 - place[q] if far else place[q]
-            send_og(q, p).wait_recv()
-            pass_og(q, p, mid).start()
-        for q in range(2):
-            p = 1 - place[q] if far else place[q]
-            pass_og(q, p, mid_other).wait_recv()
-            ogt[q, cut(p, depth), rows:2 * rows] = ogcat[q, rows:2 * rows, cut(p, depth)].T
+    def finish(q, i):
+        c = chunk(q, order[i])
+        send_pb(q, order[i]).wait_recv()
+        positive = jnp.maximum(hpc[0, c].astype(F32), 0.0)
+        hg_out[:, cut(c, fc)] = (2.0 * positive * (pbo[c] + pbr[c].astype(F32))).astype(BF)
+
+    shared = {
+        "sw": lambda q, h: send_w(q, h).start(),
+        "sog": lambda q, far: send_og(q, og_part(q, far)).start(),
+        "shp": lambda q, k: send_hp(q, k).start(),
+        "tr0": transpose_own, "ogr": og_relay, "ogt": og_whole,
+        "gout": grad_send, "gown": grad_keep, "w1": w_own,
+        "bk": back_send, "bko": back_keep, "fin": finish,
+    }
+    at_outer = {"za": z_outer_send, "zd": z_outer_last}
+    at_inner = {"zb": z_inner_send, "zc": z_inner_last, "w2a": w_down, "w2b": w_across, "w3": w_far}
+
+    def run_group(table, role, group):
+        steps = [(table[name], args) for name, *args in group if name in table]
+        if steps:
+            @pl.when(role)
+            def _():
+                for act, args in steps:
+                    act(*args)
 
     barrier = pltpu.get_barrier_semaphore()
     for peer in (apeer, bpeer, cpeer, znext, zmid):
@@ -317,74 +356,32 @@
     for q, p in both:
         load_og(q, p).start()
     pl.semaphore_wait(barrier, 5)
-    for q in range(2):
-        send_w(q).start()
-    for q in range(2):
-        send_og(q, 1 - place[q]).start()
-    for q in range(2):
-        send_hp(q, 0).start()
-    for q in range(2):
-        send_og(q, place[q]).start()
-    for k in (1, 2):
-        for q in range(2):
-            send_hp(q, k).start()
-    for c in range(2 * STEPS):
-        load_hp(c).start()
-    for c in range(2 * STEPS):
-        load_w(c).start()
-    for q, p in both:
-        load_og(q, p).wait()
-    for q in range(2):
-        ogt[q, :, 0:rows] = ogcat[q, 0:rows, :].T
-    w_first()
-    og_arrive(True)
-    for q in range(2):
-        got_hp(q, 0)
-        g_out(q, 0, act_of(q, 0))
-    w_second()
-    og_arrive(False)
-    for q in range(2):
-        g_own(q, 0, act_of(q, 0))
-    for c in range(2 * STEPS):
-        load_w(c).wait()
-    g_step(1, (3,))
-    w_third()
-    z_a(0)
-    g_step(2, (4,))
-    z_b(0)
-    z_a(1)
-    z_b(1)
-    g_step(3, ())
-    z_c(0)
-    z_a(2)
-    z_c(1)
-    z_b(2)
-    g_step(4, ())
-    back(0)
-    z_c(2)
-    z_a(3)
-    z_b(3)
-    back(1)
-    z_a(4)
-    z_c(3)
-    z_b(4)
-    back(2)
-    back(3)
-    finish(0)
-    z_c(4)
-    for k in range(count - 1):
-        z_d(k)
-    finish(1)
-    finish(2)
-    z_d(count - 1)
-    finish(3)
+    group = []
+    started = False
+    for step in PLAN:
+        if step[0] in shared:
+            run_group(at_outer, outer, group)
+            run_group(at_inner, inner, group)
+            group = []
+            if not started and step[0] == "tr0":
+                started = True
+                for c in range(2 * STEPS):
+                    load_hp(c).start()
+                for c in range(2 * STEPS):
+                    load_w(c).start()
+            shared[step[0]](*step[1:])
+        else:
+            group.append(step)
+    run_group(at_outer, outer, group)
+    run_group(at_inner, inner, group)
 
     for q, p in both:
         send_og(q, p).wait_send()
         pass_og(q, p, mid).wait_send()
     for q in range(2):
-        send_w(q).wait_send()
-        near_w(q, z).wait_send()
+        for h in range(WPARTS):
+            send_w(q, h).wait_send()
+            near_w(q, z, h).wait_send()
         for k in range(count):
             send_hp(q, k).wait_send()
         for j in range(STEPS):
@@ -401,13 +398,29 @@
     @pl.when(inner)
     def _():
         for q in range(2):
-            mid_w(q, z).wait_send()
-            mid_w(q, znear).wait_send()
-            near_w(q, last - z).wait_send()
-            near_w(q, last - znear).wait_send()
+            for h in range(WPARTS):
+                mid_w(q, z, h).wait_send()
+                mid_w(q, znear, h).wait_send()
+                near_w(q, last - z, h).wait_send()
+                near_w(q, last - znear, h).wait_send()
         for q, k, h in pieces:
             send_z2(q, k, h).wait_send()
             send_z3(q, k, h).wait_send()
+
+
+def put_kernel(hg, total, hg_out, tot_out, wide, sems):
+    size = hg.shape[0] // PUTS
+    tokens_all = size * PUTS * lax.axis_size("rep") * lax.axis_size("fs")
+    copies = []
+    for i in range(PUTS):
+        span = pl.ds(i * size, size)
+        copies.append(pltpu.make_async_copy(hg.at[span], hg_out.at[span], sems.at[1, i]))
+        copies[-1].start()
+        wide[span] = total[span].astype(F32) * (1.0 / math.sqrt(tokens_all))
+        copies.append(pltpu.make_async_copy(wide.at[span], tot_out.at[span], sems.at[0, i]))
+        copies[-1].start()
+    for copy in copies:
+        copy.wait()
 
 
 def paired_body(hidden_pre, out_grad, down_weight):
@@ -437,14 +450,20 @@
             block(depth, BF), block(depth, BF), block(depth, F32),
             block(depth, BF), block(depth, BF), block(depth, BF), block(depth, BF),
             sem((2, 2)), sem((chunks,)), sem((chunks,)),
-        ] + [sem((2, 2))] * 4 + [sem((2,))] * 2 + [sem((chunks,))] * 5
-        + [sem((2, count))] * 2 + [sem((2, count, 2))] * 8,
+        ] + [sem((2, 2))] * 4 + [sem((2, WPARTS))] * 2 + [sem((chunks, WPARTS))] * 3 + [sem((chunks,))] * 2
+        + [sem((2, count))] * 2 + [sem((2, count, PARTS))] * 8,
         compiler_params=pltpu.CompilerParams(
             collective_id=0, has_side_effects=True, vmem_limit_bytes=48 * 1024 * 1024
         ),
     )(hidden_pre, out_grad, down_weight)
-    tokens_all = rows * lax.axis_size("rep") * lax.axis_size("fs")
-    return hidden_grad, total.astype(F32) * (1.0 / math.sqrt(tokens_all))
+    return pl.pallas_call(
+        put_kernel,
+        out_shape=(jax.ShapeDtypeStruct((rows, ff), BF), jax.ShapeDtypeStruct((depth, ff), F32)),
+        in_specs=[any_spec, vmem_spec],
+        out_specs=(any_spec, any_spec),
+        scratch_shapes=[pltpu.VMEM((depth, ff), F32), pltpu.SemaphoreType.DMA((2, PUTS))],
+        compiler_params=pltpu.CompilerParams(vmem_limit_bytes=8 * 1024 * 1024),
+    )(hidden_grad, total)
 
 
 def solution(mesh):

time: 109 us -> 100 us (0.917)
  Pallas kernels: 105 us -> 99.5 us
  other arithmetic: 2.59 us -> 0 us
  local copies, waits for them, and re-layouts: 1.32 us -> 0 us
    pallas_call x1, Pallas kernels: 105 us -> 96.8 us  [paired_body(): pl.pallas_call(kernel, out_shape=(jax.ShapeDtypeStruct((rows, ff), BF), j...]
    pallas_call x0 -> x1, Pallas kernels: none -> 2.75 us  [paired_body(): pl.pallas_call(put_kernel, out_shape=(jax.ShapeDtypeStruct((rows, ff), BF...]
    mul x1 -> x0, other arithmetic: 2.59 us -> none  [paired_body(): return (hidden_grad, total.astype(F32) * (1.0 / math.sqrt(tokens_all)))]
    unnamed x1 -> x0, local copies, waits for them, and re-layouts: 1.32 us -> none
where the time goes in v2:
time: 100 us
  Pallas kernels  99.5 us (100%)
    pallas_call x1, Pallas kernels, paired_body(): pl.pallas_call(kernel, out_shape=(jax.ShapeDtypeStruct((rows, ff), BF), j...  96.8 us
    pallas_call x1, Pallas kernels, paired_body(): pl.pallas_call(put_kernel, out_shape=(jax.ShapeDtypeStruct((rows, ff), BF...  2.75 us

profile of v2, /device:TPU:0, one launch (start us, length us, event | category | flops | bytes accessed | tf_op | source)
XLA Modules:
  0.0 100.3 jit_solution(12351301106137787481)
XLA Ops:
  0.6 96.8 %shard_map.50 = (bf16[512,2048]{1,0:T(8,128)(2,1)S(1)}, bf16[512,2048]{1,0:T(8,128)(2,1)S(1)}) custom-call(bf16[512,2048]{1,0:T(8,128)(2,1)} %hp.1, bf16[512,2048]{1,0:T(8,128)(2,1)} %og.1, bf16[512,2048]{1,0:T(8,128)(2,1)} %w.1), custom_call_target="tpu_custom_call" | custom-call | tf_op jit(solution)/shard_map/pallas_call | solution.py:439
  97.4 2.8 %shard_map.51 = (bf16[512,2048]{1,0:T(8,128)(2,1)}, f32[512,2048]{1,0:T(8,128)}) custom-call(bf16[512,2048]{1,0:T(8,128)(2,1)S(1)} %get-tuple-element.4.hg, bf16[512,2048]{1,0:T(8,128)(2,1)S(1)} %get-tuple-element.5.total), custom_call_target="tpu_custom_call" | custom-call | tf_op jit(solution)/shard_map/pallas_call | solution.py:459

commit v3 on v2

--- a/solution.py
+++ b/solution.py
@@ -38,39 +38,35 @@
 
 
 STEPS = 4
-PIECES = ((0, 0, 1), (0, 1, 1), (1, 0, 2), (2, 0, 2), (3, 0, 2))
-PUTS = 4
+PIECES = ((0, 0, 2), (1, 0, 2), (2, 0, 2), (3, 0, 2))
+PUTS = 2
 PARTS = 2
 WPARTS = 2
 PLAN = (
-    ("sw", 1, 0), ("sw", 0, 1), ("sw", 0, 0), ("sw", 1, 1), ("sog", 0, 1), ("sog", 0, 0), ("sog", 1, 1),
-    ("w1", 1, 0), ("tr0", 1), ("w1", 0, 0), ("shp", 0, 3), ("sog", 1, 0), ("w2b", 1, 0), ("w1", 1, 1),
-    ("shp", 0, 1), ("shp", 1, 1), ("w2a", 1, 0), ("w2b", 1, 1), ("w3", 1, 0), ("w1", 0, 1), ("w2a", 0, 0),
-    ("shp", 1, 2), ("ogr", 1, 1), ("ogr", 0, 1), ("tr0", 0), ("w2b", 0, 1), ("ogr", 1, 0), ("ogr", 0, 0),
-    ("w2a", 1, 1), ("ogt", 0, 1), ("ogt", 1, 1), ("shp", 0, 0), ("gout", 1, 1), ("ogt", 0, 0),
-    ("gout", 0, 3), ("shp", 0, 2), ("w3", 1, 1), ("w2a", 0, 1), ("w2b", 0, 0), ("gown", 0, 3),
-    ("gout", 1, 2), ("gout", 0, 1), ("shp", 0, 4), ("ogt", 1, 0), ("w3", 0, 0), ("za", 0, 3, 0),
-    ("gout", 0, 0), ("za", 0, 3, 1), ("w3", 0, 1), ("shp", 1, 0), ("shp", 1, 3), ("zb", 0, 3, 0),
-    ("zb", 0, 3, 1), ("gown", 0, 1), ("zc", 0, 3, 0), ("gown", 1, 1), ("za", 0, 1, 0), ("za", 0, 1, 1),
-    ("za", 1, 1, 0), ("za", 1, 1, 1), ("zb", 0, 1, 0), ("zb", 0, 1, 1), ("gown", 1, 2), ("gout", 0, 2),
-    ("zb", 1, 1, 1), ("shp", 1, 4), ("za", 1, 2, 0), ("za", 1, 2, 1), ("zb", 1, 1, 0), ("zc", 0, 3, 1),
-    ("gown", 0, 0), ("zb", 1, 2, 0), ("zc", 0, 1, 1), ("gown", 0, 2), ("gout", 1, 0), ("za", 0, 0, 0),
-    ("gout", 1, 3), ("za", 0, 0, 1), ("za", 0, 2, 0), ("zc", 1, 1, 1), ("bk", 0, 2), ("gown", 1, 0),
-    ("zc", 1, 1, 0), ("zd", 0, 1, 1), ("za", 1, 0, 1), ("zd", 1, 1, 0), ("zb", 1, 2, 1), ("zc", 0, 1, 0),
-    ("gown", 1, 3), ("za", 0, 2, 1), ("zc", 1, 2, 0), ("zb", 0, 0, 0), ("gout", 0, 4), ("zd", 0, 3, 1),
-    ("zb", 0, 0, 1), ("zc", 1, 2, 1), ("bk", 1, 0), ("zb", 0, 2, 0), ("zb", 1, 0, 1), ("za", 1, 3, 0),
-    ("zc", 0, 0, 1), ("bko", 0, 2), ("zc", 0, 0, 0), ("zb", 0, 2, 1), ("gout", 1, 4), ("za", 1, 3, 1),
-    ("za", 1, 0, 0), ("zc", 0, 2, 0), ("zb", 1, 3, 0), ("zc", 0, 2, 1), ("bko", 1, 0), ("gown", 0, 4),
-    ("gown", 1, 4), ("za", 0, 4, 1), ("za", 0, 4, 0), ("zd", 0, 2, 0), ("zb", 1, 3, 1), ("bk", 0, 1),
-    ("bk", 1, 1), ("zc", 1, 0, 1), ("bk", 1, 3), ("bk", 0, 0), ("zc", 1, 3, 0), ("bko", 0, 1),
-    ("zb", 0, 4, 1), ("za", 1, 4, 0), ("bko", 1, 1), ("zd", 0, 0, 1), ("za", 1, 4, 1), ("zc", 1, 3, 1),
-    ("zd", 1, 0, 1), ("zb", 0, 4, 0), ("zd", 1, 3, 1), ("bk", 1, 2), ("zc", 0, 4, 1), ("zb", 1, 4, 0),
-    ("zd", 0, 1, 0), ("bko", 1, 3), ("bk", 0, 3), ("fin", 1, 0), ("bko", 0, 3), ("zc", 0, 4, 0),
-    ("zd", 0, 3, 0), ("bko", 0, 0), ("zb", 1, 4, 1), ("fin", 1, 1), ("bko", 1, 2), ("zb", 1, 0, 0),
-    ("zc", 1, 4, 0), ("zd", 0, 0, 0), ("fin", 1, 3), ("zc", 1, 4, 1), ("zd", 0, 2, 1), ("fin", 0, 2),
-    ("fin", 0, 1), ("fin", 0, 0), ("zd", 1, 4, 1), ("zd", 1, 2, 1), ("zc", 1, 0, 0), ("zd", 1, 1, 1),
-    ("zd", 1, 3, 0), ("zd", 0, 4, 0), ("zd", 1, 4, 0), ("fin", 0, 3), ("zd", 1, 2, 0), ("fin", 1, 2),
-    ("zd", 0, 4, 1), ("zd", 1, 0, 0),
+    ("sw", 0, 1), ("sw", 0, 0), ("sw", 1, 1), ("sog", 0, 1), ("sog", 1, 1), ("sw", 1, 0), ("sog", 1, 0),
+    ("shp", 0, 3), ("w1", 1, 1), ("sog", 0, 0), ("w1", 0, 0), ("tr0", 0), ("ogr", 0, 1), ("w2b", 1, 1),
+    ("shp", 0, 2), ("w1", 0, 1), ("shp", 1, 2), ("w1", 1, 0), ("w2b", 0, 0), ("w2a", 1, 1), ("ogr", 1, 1),
+    ("w2b", 0, 1), ("ogt", 1, 1), ("w2a", 0, 0), ("w2b", 1, 0), ("ogt", 0, 1), ("ogr", 1, 0), ("w2a", 0, 1),
+    ("gout", 0, 3), ("w2a", 1, 0), ("shp", 1, 0), ("ogr", 0, 0), ("tr0", 1), ("ogt", 1, 0), ("gout", 1, 2),
+    ("w3", 0, 0), ("w3", 1, 1), ("w3", 1, 0), ("ogt", 0, 0), ("gown", 0, 3), ("shp", 0, 1), ("zb", 0, 3, 0),
+    ("za", 0, 3, 0), ("za", 0, 3, 1), ("w3", 0, 1), ("gout", 0, 2), ("zb", 0, 3, 1), ("gown", 0, 2),
+    ("shp", 1, 3), ("gown", 1, 2), ("za", 1, 2, 0), ("za", 1, 2, 1), ("gout", 1, 0), ("zc", 0, 3, 0),
+    ("zb", 1, 2, 0), ("za", 0, 2, 0), ("za", 0, 2, 1), ("gown", 1, 0), ("zb", 1, 2, 1), ("zc", 0, 3, 1),
+    ("zc", 1, 2, 0), ("zb", 0, 2, 0), ("shp", 0, 0), ("gout", 0, 1), ("gown", 0, 1), ("za", 1, 0, 0),
+    ("zc", 1, 2, 1), ("zb", 0, 2, 1), ("shp", 1, 1), ("za", 1, 0, 1), ("gout", 1, 3), ("zc", 0, 2, 0),
+    ("za", 0, 1, 0), ("zb", 1, 0, 0), ("bk", 0, 2), ("gown", 1, 3), ("zc", 0, 2, 1), ("zb", 1, 0, 1),
+    ("za", 0, 1, 1), ("gout", 0, 0), ("bk", 1, 1), ("za", 1, 3, 0), ("bk", 1, 3), ("gown", 0, 0),
+    ("zc", 1, 0, 0), ("za", 1, 3, 1), ("zb", 0, 1, 0), ("bko", 1, 1), ("zd", 0, 3, 1), ("bk", 1, 0),
+    ("zb", 0, 1, 1), ("zc", 1, 0, 1), ("zd", 1, 2, 1), ("gout", 1, 1), ("gown", 1, 1), ("bk", 0, 1),
+    ("za", 0, 0, 0), ("bko", 0, 2), ("zc", 0, 1, 0), ("zb", 1, 3, 0), ("bk", 0, 0), ("zb", 1, 3, 1),
+    ("zc", 0, 1, 1), ("zc", 1, 3, 0), ("za", 0, 0, 1), ("zb", 0, 0, 0), ("za", 1, 1, 0), ("za", 1, 1, 1),
+    ("zb", 0, 0, 1), ("zc", 1, 3, 1), ("zc", 0, 0, 0), ("zd", 1, 0, 0), ("fin", 0, 2), ("zb", 1, 1, 0),
+    ("bk", 1, 2), ("bko", 0, 1), ("zc", 0, 0, 1), ("zb", 1, 1, 1), ("bk", 0, 3), ("zd", 0, 2, 1),
+    ("zd", 1, 3, 1), ("bko", 1, 3), ("zd", 1, 0, 1), ("zc", 1, 1, 0), ("zd", 1, 3, 0), ("zd", 0, 1, 0),
+    ("zd", 0, 3, 0), ("bko", 1, 0), ("zc", 1, 1, 1), ("zd", 1, 2, 0), ("bko", 0, 3), ("zd", 0, 0, 1),
+    ("zd", 0, 0, 0), ("fin", 1, 0), ("zd", 0, 1, 1), ("bko", 0, 0), ("fin", 0, 1), ("fin", 1, 3),
+    ("fin", 1, 1), ("bko", 1, 2), ("zd", 0, 2, 0), ("zd", 1, 1, 1), ("fin", 0, 0), ("zd", 1, 1, 0),
+    ("fin", 1, 2), ("fin", 0, 3),
 )
 
 

time: 100 us -> 97.8 us (0.978)
  Pallas kernels: 99.5 us -> 96.9 us
    pallas_call x1, Pallas kernels: 96.8 us -> 94.1 us  [paired_body(): pl.pallas_call(kernel, out_shape=(jax.ShapeDtypeStruct((rows, ff), BF), j...]
where the time goes in v3:
time: 97.8 us; the launch traced here: 97.7 us
  Pallas kernels  96.9 us (99%)
    pallas_call x1, Pallas kernels, paired_body(): pl.pallas_call(kernel, out_shape=(jax.ShapeDtypeStruct((rows, ff), BF), j...  94.1 us
    pallas_call x1, Pallas kernels, paired_body(): pl.pallas_call(put_kernel, out_shape=(jax.ShapeDtypeStruct((rows, ff), BF...  2.74 us

profile of v3, /device:TPU:0, one launch (start us, length us, event | category | flops | bytes accessed | tf_op | source)
XLA Modules:
  0.0 97.7 jit_solution(14443714030112810166)
XLA Ops:
  0.6 94.1 %shard_map.50 = (bf16[512,2048]{1,0:T(8,128)(2,1)S(1)}, bf16[512,2048]{1,0:T(8,128)(2,1)S(1)}) custom-call(bf16[512,2048]{1,0:T(8,128)(2,1)} %hp.1, bf16[512,2048]{1,0:T(8,128)(2,1)} %og.1, bf16[512,2048]{1,0:T(8,128)(2,1)} %w.1), custom_call_target="tpu_custom_call" | custom-call | tf_op jit(solution)/shard_map/pallas_call | solution.py:435
  94.8 2.7 %shard_map.51 = (bf16[512,2048]{1,0:T(8,128)(2,1)}, f32[512,2048]{1,0:T(8,128)}) custom-call(bf16[512,2048]{1,0:T(8,128)(2,1)S(1)} %get-tuple-element.4.hg, bf16[512,2048]{1,0:T(8,128)(2,1)S(1)} %get-tuple-element.5.total), custom_call_target="tpu_custom_call" | custom-call | tf_op jit(solution)/shard_map/pallas_call | solution.py:455

commit v4 on v3

--- a/solution.py
+++ b/solution.py
@@ -39,34 +39,34 @@
 
 STEPS = 4
 PIECES = ((0, 0, 2), (1, 0, 2), (2, 0, 2), (3, 0, 2))
-PUTS = 2
+PUTS = 4
 PARTS = 2
 WPARTS = 2
 PLAN = (
-    ("sw", 0, 1), ("sw", 0, 0), ("sw", 1, 1), ("sog", 0, 1), ("sog", 1, 1), ("sw", 1, 0), ("sog", 1, 0),
-    ("shp", 0, 3), ("w1", 1, 1), ("sog", 0, 0), ("w1", 0, 0), ("tr0", 0), ("ogr", 0, 1), ("w2b", 1, 1),
-    ("shp", 0, 2), ("w1", 0, 1), ("shp", 1, 2), ("w1", 1, 0), ("w2b", 0, 0), ("w2a", 1, 1), ("ogr", 1, 1),
-    ("w2b", 0, 1), ("ogt", 1, 1), ("w2a", 0, 0), ("w2b", 1, 0), ("ogt", 0, 1), ("ogr", 1, 0), ("w2a", 0, 1),
-    ("gout", 0, 3), ("w2a", 1, 0), ("shp", 1, 0), ("ogr", 0, 0), ("tr0", 1), ("ogt", 1, 0), ("gout", 1, 2),
-    ("w3", 0, 0), ("w3", 1, 1), ("w3", 1, 0), ("ogt", 0, 0), ("gown", 0, 3), ("shp", 0, 1), ("zb", 0, 3, 0),
-    ("za", 0, 3, 0), ("za", 0, 3, 1), ("w3", 0, 1), ("gout", 0, 2), ("zb", 0, 3, 1), ("gown", 0, 2),
-    ("shp", 1, 3), ("gown", 1, 2), ("za", 1, 2, 0), ("za", 1, 2, 1), ("gout", 1, 0), ("zc", 0, 3, 0),
-    ("zb", 1, 2, 0), ("za", 0, 2, 0), ("za", 0, 2, 1), ("gown", 1, 0), ("zb", 1, 2, 1), ("zc", 0, 3, 1),
-    ("zc", 1, 2, 0), ("zb", 0, 2, 0), ("shp", 0, 0), ("gout", 0, 1), ("gown", 0, 1), ("za", 1, 0, 0),
-    ("zc", 1, 2, 1), ("zb", 0, 2, 1), ("shp", 1, 1), ("za", 1, 0, 1), ("gout", 1, 3), ("zc", 0, 2, 0),
-    ("za", 0, 1, 0), ("zb", 1, 0, 0), ("bk", 0, 2), ("gown", 1, 3), ("zc", 0, 2, 1), ("zb", 1, 0, 1),
-    ("za", 0, 1, 1), ("gout", 0, 0), ("bk", 1, 1), ("za", 1, 3, 0), ("bk", 1, 3), ("gown", 0, 0),
-    ("zc", 1, 0, 0), ("za", 1, 3, 1), ("zb", 0, 1, 0), ("bko", 1, 1), ("zd", 0, 3, 1), ("bk", 1, 0),
-    ("zb", 0, 1, 1), ("zc", 1, 0, 1), ("zd", 1, 2, 1), ("gout", 1, 1), ("gown", 1, 1), ("bk", 0, 1),
-    ("za", 0, 0, 0), ("bko", 0, 2), ("zc", 0, 1, 0), ("zb", 1, 3, 0), ("bk", 0, 0), ("zb", 1, 3, 1),
-    ("zc", 0, 1, 1), ("zc", 1, 3, 0), ("za", 0, 0, 1), ("zb", 0, 0, 0), ("za", 1, 1, 0), ("za", 1, 1, 1),
-    ("zb", 0, 0, 1), ("zc", 1, 3, 1), ("zc", 0, 0, 0), ("zd", 1, 0, 0), ("fin", 0, 2), ("zb", 1, 1, 0),
-    ("bk", 1, 2), ("bko", 0, 1), ("zc", 0, 0, 1), ("zb", 1, 1, 1), ("bk", 0, 3), ("zd", 0, 2, 1),
-    ("zd", 1, 3, 1), ("bko", 1, 3), ("zd", 1, 0, 1), ("zc", 1, 1, 0), ("zd", 1, 3, 0), ("zd", 0, 1, 0),
-    ("zd", 0, 3, 0), ("bko", 1, 0), ("zc", 1, 1, 1), ("zd", 1, 2, 0), ("bko", 0, 3), ("zd", 0, 0, 1),
-    ("zd", 0, 0, 0), ("fin", 1, 0), ("zd", 0, 1, 1), ("bko", 0, 0), ("fin", 0, 1), ("fin", 1, 3),
-    ("fin", 1, 1), ("bko", 1, 2), ("zd", 0, 2, 0), ("zd", 1, 1, 1), ("fin", 0, 0), ("zd", 1, 1, 0),
-    ("fin", 1, 2), ("fin", 0, 3),
+    ("sw", 1, 1), ("sw", 1, 0), ("sw", 0, 0), ("sw", 0, 1), ("tr0", 0), ("sog", 1, 1), ("w1", 0, 0),
+    ("sog", 0, 1), ("w1", 1, 0), ("w2b", 0, 0), ("sog", 1, 0), ("w1", 0, 1), ("shp", 0, 0), ("sog", 0, 0),
+    ("w1", 1, 1), ("ogr", 0, 1), ("shp", 1, 3), ("ogr", 1, 1), ("ogt", 1, 1), ("ogt", 0, 1), ("w2b", 1, 0),
+    ("w2a", 0, 0), ("tr0", 1), ("w2b", 1, 1), ("w2a", 0, 1), ("w2a", 1, 0), ("gout", 0, 0), ("w2b", 0, 1),
+    ("shp", 0, 2), ("ogr", 1, 0), ("w2a", 1, 1), ("shp", 1, 2), ("w3", 0, 0), ("ogr", 0, 0), ("gout", 1, 3),
+    ("ogt", 0, 0), ("w3", 1, 0), ("shp", 0, 1), ("gown", 0, 0), ("ogt", 1, 0), ("za", 0, 0, 0), ("w3", 1, 1),
+    ("za", 0, 0, 1), ("gown", 1, 3), ("gout", 0, 2), ("shp", 1, 0), ("za", 1, 3, 0), ("zb", 0, 0, 0),
+    ("gown", 0, 2), ("w3", 0, 1), ("za", 1, 3, 1), ("zb", 0, 0, 1), ("gout", 1, 2), ("zb", 1, 3, 0),
+    ("za", 0, 2, 0), ("za", 0, 2, 1), ("zc", 0, 0, 0), ("zb", 1, 3, 1), ("zc", 0, 0, 1), ("gown", 1, 2),
+    ("shp", 0, 3), ("zb", 0, 2, 0), ("zc", 1, 3, 0), ("za", 1, 2, 0), ("gout", 0, 1), ("za", 1, 2, 1),
+    ("gown", 0, 1), ("shp", 1, 1), ("zb", 0, 2, 1), ("zc", 1, 3, 1), ("za", 0, 1, 0), ("gout", 1, 0),
+    ("zb", 1, 2, 0), ("bk", 0, 3), ("zc", 0, 2, 0), ("za", 0, 1, 1), ("zb", 1, 2, 1), ("gown", 1, 0),
+    ("zc", 0, 2, 1), ("zb", 0, 1, 0), ("zc", 1, 2, 0), ("gout", 0, 3), ("bk", 1, 2), ("zb", 0, 1, 1),
+    ("za", 1, 0, 0), ("gown", 0, 3), ("zc", 1, 2, 1), ("za", 1, 0, 1), ("zb", 1, 0, 0), ("zd", 1, 3, 1),
+    ("zc", 0, 1, 0), ("gout", 1, 1), ("zb", 1, 0, 1), ("za", 0, 3, 0), ("zd", 0, 2, 1), ("bk", 1, 1),
+    ("zc", 0, 1, 1), ("gown", 1, 1), ("bk", 0, 1), ("zb", 0, 3, 0), ("za", 0, 3, 1), ("bko", 0, 1),
+    ("zd", 1, 2, 1), ("zc", 1, 0, 0), ("zb", 0, 3, 1), ("za", 1, 1, 0), ("bk", 1, 0), ("zd", 0, 0, 0),
+    ("zd", 1, 3, 0), ("za", 1, 1, 1), ("zc", 1, 0, 1), ("zb", 1, 1, 0), ("zc", 0, 3, 0), ("bk", 0, 2),
+    ("bko", 0, 3), ("bko", 1, 2), ("zb", 1, 1, 1), ("zc", 0, 3, 1), ("bk", 1, 3), ("bko", 1, 1),
+    ("bk", 0, 0), ("zc", 1, 1, 0), ("zd", 0, 2, 0), ("fin", 0, 1), ("bko", 1, 3), ("zd", 1, 2, 0),
+    ("zd", 1, 0, 0), ("fin", 0, 3), ("bko", 1, 0), ("zc", 1, 1, 1), ("fin", 1, 2), ("zd", 1, 0, 1),
+    ("bko", 0, 0), ("zd", 0, 1, 1), ("bko", 0, 2), ("zd", 0, 0, 1), ("zd", 0, 1, 0), ("zd", 0, 3, 1),
+    ("zd", 1, 1, 0), ("fin", 0, 2), ("zd", 0, 3, 0), ("fin", 1, 1), ("fin", 1, 0), ("fin", 1, 3),
+    ("fin", 0, 0), ("zd", 1, 1, 1),
 )
 
 
@@ -347,11 +347,16 @@
                     act(*args)
 
     barrier = pltpu.get_barrier_semaphore()
-    for peer in (apeer, bpeer, cpeer, znext, zmid):
+    for peer in (apeer, bpeer, cpeer, znext):
         pl.semaphore_signal(barrier, inc=1, device_id=peer, device_id_type=MESH)
+
+    @pl.when(inner)
+    def _():
+        pl.semaphore_signal(barrier, inc=1, device_id=zmid, device_id_type=MESH)
+
     for q, p in both:
         load_og(q, p).start()
-    pl.semaphore_wait(barrier, 5)
+    pl.semaphore_wait(barrier, jnp.where(outer, 4, 5))
     group = []
     started = False
     for step in PLAN:

time: 97.8 us -> 96.1 us (0.983)
  Pallas kernels: 96.9 us -> 95.2 us
    pallas_call x1, Pallas kernels: 94.1 us -> 92.4 us  [paired_body(): pl.pallas_call(kernel, out_shape=(jax.ShapeDtypeStruct((rows, ff), BF), j...]
where the time goes in v4:
time: 96.1 us; the launch traced here: 96 us
  Pallas kernels  95.2 us (99%)
    pallas_call x1, Pallas kernels, paired_body(): pl.pallas_call(kernel, out_shape=(jax.ShapeDtypeStruct((rows, ff), BF), j...  92.4 us
    pallas_call x1, Pallas kernels, paired_body(): pl.pallas_call(put_kernel, out_shape=(jax.ShapeDtypeStruct((rows, ff), BF...  2.75 us

profile of v4, /device:TPU:0, one launch (start us, length us, event | category | flops | bytes accessed | tf_op | source)
XLA Modules:
  0.0 96.0 jit_solution(17160285869912264290)
XLA Ops:
  0.6 92.4 %shard_map.50 = (bf16[512,2048]{1,0:T(8,128)(2,1)S(1)}, bf16[512,2048]{1,0:T(8,128)(2,1)S(1)}) custom-call(bf16[512,2048]{1,0:T(8,128)(2,1)} %hp.1, bf16[512,2048]{1,0:T(8,128)(2,1)} %og.1, bf16[512,2048]{1,0:T(8,128)(2,1)} %w.1), custom_call_target="tpu_custom_call" | custom-call | tf_op jit(solution)/shard_map/pallas_call | solution.py:440
  93.1 2.8 %shard_map.51 = (bf16[512,2048]{1,0:T(8,128)(2,1)}, f32[512,2048]{1,0:T(8,128)}) custom-call(bf16[512,2048]{1,0:T(8,128)(2,1)S(1)} %get-tuple-element.4.hg, bf16[512,2048]{1,0:T(8,128)(2,1)S(1)} %get-tuple-element.5.total), custom_call_target="tpu_custom_call" | custom-call | tf_op jit(solution)/shard_map/pallas_call | solution.py:460

commit v5 on v4

--- a/solution.py
+++ b/solution.py
@@ -38,50 +38,58 @@
 
 
 STEPS = 4
-PIECES = ((0, 0, 2), (1, 0, 2), (2, 0, 2), (3, 0, 2))
-PUTS = 4
+PIECES = ((0, 0, 2), (1, 0, 1), (1, 1, 1), (2, 0, 2), (3, 0, 2))
+SHIFT = 16
+PUTS = 2
 PARTS = 2
-WPARTS = 2
+VIA_Z = 1
 PLAN = (
-    ("sw", 1, 1), ("sw", 1, 0), ("sw", 0, 0), ("sw", 0, 1), ("tr0", 0), ("sog", 1, 1), ("w1", 0, 0),
-    ("sog", 0, 1), ("w1", 1, 0), ("w2b", 0, 0), ("sog", 1, 0), ("w1", 0, 1), ("shp", 0, 0), ("sog", 0, 0),
-    ("w1", 1, 1), ("ogr", 0, 1), ("shp", 1, 3), ("ogr", 1, 1), ("ogt", 1, 1), ("ogt", 0, 1), ("w2b", 1, 0),
-    ("w2a", 0, 0), ("tr0", 1), ("w2b", 1, 1), ("w2a", 0, 1), ("w2a", 1, 0), ("gout", 0, 0), ("w2b", 0, 1),
-    ("shp", 0, 2), ("ogr", 1, 0), ("w2a", 1, 1), ("shp", 1, 2), ("w3", 0, 0), ("ogr", 0, 0), ("gout", 1, 3),
-    ("ogt", 0, 0), ("w3", 1, 0), ("shp", 0, 1), ("gown", 0, 0), ("ogt", 1, 0), ("za", 0, 0, 0), ("w3", 1, 1),
-    ("za", 0, 0, 1), ("gown", 1, 3), ("gout", 0, 2), ("shp", 1, 0), ("za", 1, 3, 0), ("zb", 0, 0, 0),
-    ("gown", 0, 2), ("w3", 0, 1), ("za", 1, 3, 1), ("zb", 0, 0, 1), ("gout", 1, 2), ("zb", 1, 3, 0),
-    ("za", 0, 2, 0), ("za", 0, 2, 1), ("zc", 0, 0, 0), ("zb", 1, 3, 1), ("zc", 0, 0, 1), ("gown", 1, 2),
-    ("shp", 0, 3), ("zb", 0, 2, 0), ("zc", 1, 3, 0), ("za", 1, 2, 0), ("gout", 0, 1), ("za", 1, 2, 1),
-    ("gown", 0, 1), ("shp", 1, 1), ("zb", 0, 2, 1), ("zc", 1, 3, 1), ("za", 0, 1, 0), ("gout", 1, 0),
-    ("zb", 1, 2, 0), ("bk", 0, 3), ("zc", 0, 2, 0), ("za", 0, 1, 1), ("zb", 1, 2, 1), ("gown", 1, 0),
-    ("zc", 0, 2, 1), ("zb", 0, 1, 0), ("zc", 1, 2, 0), ("gout", 0, 3), ("bk", 1, 2), ("zb", 0, 1, 1),
-    ("za", 1, 0, 0), ("gown", 0, 3), ("zc", 1, 2, 1), ("za", 1, 0, 1), ("zb", 1, 0, 0), ("zd", 1, 3, 1),
-    ("zc", 0, 1, 0), ("gout", 1, 1), ("zb", 1, 0, 1), ("za", 0, 3, 0), ("zd", 0, 2, 1), ("bk", 1, 1),
-    ("zc", 0, 1, 1), ("gown", 1, 1), ("bk", 0, 1), ("zb", 0, 3, 0), ("za", 0, 3, 1), ("bko", 0, 1),
-    ("zd", 1, 2, 1), ("zc", 1, 0, 0), ("zb", 0, 3, 1), ("za", 1, 1, 0), ("bk", 1, 0), ("zd", 0, 0, 0),
-    ("zd", 1, 3, 0), ("za", 1, 1, 1), ("zc", 1, 0, 1), ("zb", 1, 1, 0), ("zc", 0, 3, 0), ("bk", 0, 2),
-    ("bko", 0, 3), ("bko", 1, 2), ("zb", 1, 1, 1), ("zc", 0, 3, 1), ("bk", 1, 3), ("bko", 1, 1),
-    ("bk", 0, 0), ("zc", 1, 1, 0), ("zd", 0, 2, 0), ("fin", 0, 1), ("bko", 1, 3), ("zd", 1, 2, 0),
-    ("zd", 1, 0, 0), ("fin", 0, 3), ("bko", 1, 0), ("zc", 1, 1, 1), ("fin", 1, 2), ("zd", 1, 0, 1),
-    ("bko", 0, 0), ("zd", 0, 1, 1), ("bko", 0, 2), ("zd", 0, 0, 1), ("zd", 0, 1, 0), ("zd", 0, 3, 1),
-    ("zd", 1, 1, 0), ("fin", 0, 2), ("zd", 0, 3, 0), ("fin", 1, 1), ("fin", 1, 0), ("fin", 1, 3),
-    ("fin", 0, 0), ("zd", 1, 1, 1),
+    ("sw2", 1), ("sw1", 0), ("sw1", 1), ("sw", 0), ("w1c", 1), ("tr0", 0), ("sog", 1, 1), ("sw", 1),
+    ("tr0", 1), ("w1b", 0), ("w1b", 1), ("sog", 0, 1), ("w1", 1), ("shp", 0, 1), ("w1", 0), ("sw2", 0),
+    ("w4", 1), ("sog", 0, 0), ("shp", 1, 1), ("sog", 1, 0), ("w2b", 0, 1), ("ogr", 1, 1), ("w1c", 0),
+    ("w2b", 1, 1), ("w2a", 1, 1), ("shp", 1, 2), ("ogr", 0, 1), ("w2a", 1, 0), ("ogt", 1, 1), ("shp", 0, 3),
+    ("gout", 1, 1), ("ogt", 0, 1), ("shp", 1, 0), ("w2a", 0, 0), ("w3", 0, 1), ("w2b", 0, 0), ("w2b", 1, 0),
+    ("w2a", 0, 1), ("zg", 1, 1, 0), ("gout", 0, 1), ("ogr", 1, 0), ("ogr", 0, 0), ("ogt", 1, 0),
+    ("ogt", 0, 0), ("gown", 0, 1), ("gown", 1, 1), ("zg", 1, 1, 1), ("za", 1, 1, 0), ("za", 0, 1, 1),
+    ("w3", 0, 0), ("gout", 1, 2), ("shp", 0, 2), ("zg", 0, 1, 0), ("za", 1, 1, 1), ("zg", 0, 1, 1),
+    ("za", 0, 1, 0), ("w4", 0), ("gout", 0, 3), ("w3", 1, 0), ("w2a", 1, 2), ("zb", 1, 1, 0), ("gown", 1, 2),
+    ("za", 1, 2, 1), ("gout", 1, 0), ("za", 1, 2, 0), ("w2a", 0, 2), ("gown", 0, 3), ("zb", 0, 1, 1),
+    ("zc", 1, 1, 0), ("w3", 1, 1), ("zb", 1, 1, 1), ("shp", 1, 4), ("za", 0, 3, 0), ("zb", 1, 2, 1),
+    ("zb", 1, 2, 0), ("gown", 1, 0), ("shp", 0, 4), ("gout", 0, 2), ("gown", 0, 2), ("zc", 1, 1, 1),
+    ("zb", 0, 1, 0), ("zb", 0, 3, 0), ("za", 0, 3, 1), ("zc", 0, 1, 1), ("za", 1, 0, 0), ("zc", 1, 2, 1),
+    ("shp", 1, 3), ("zc", 0, 1, 0), ("zb", 0, 3, 1), ("za", 1, 0, 1), ("gout", 1, 4), ("zc", 1, 2, 0),
+    ("za", 0, 2, 0), ("shp", 0, 0), ("zc", 0, 3, 0), ("zb", 1, 0, 0), ("zb", 1, 0, 1), ("gout", 0, 4),
+    ("zc", 0, 3, 1), ("zb", 0, 2, 0), ("zc", 1, 0, 0), ("zb", 0, 2, 1), ("za", 0, 2, 1), ("gown", 0, 4),
+    ("gown", 1, 4), ("za", 1, 4, 0), ("bk", 1, 0), ("zd", 1, 1, 1), ("zc", 1, 0, 1), ("zb", 1, 4, 0),
+    ("za", 1, 4, 1), ("gout", 1, 3), ("zc", 0, 2, 0), ("bk", 0, 3), ("zd", 1, 2, 0), ("bk", 0, 0),
+    ("za", 0, 4, 0), ("zc", 0, 2, 1), ("bk", 0, 1), ("zb", 1, 4, 1), ("zd", 0, 1, 0), ("bko", 1, 0),
+    ("gown", 1, 3), ("za", 0, 4, 1), ("zd", 1, 2, 1), ("zc", 1, 4, 0), ("gout", 0, 0), ("zb", 0, 4, 0),
+    ("bko", 0, 3), ("bk", 1, 1), ("za", 1, 3, 0), ("zc", 1, 4, 1), ("zb", 0, 4, 1), ("gown", 0, 0),
+    ("bk", 0, 2), ("za", 1, 3, 1), ("zb", 1, 3, 0), ("zd", 0, 3, 1), ("bko", 0, 0), ("zc", 0, 4, 0),
+    ("bko", 1, 1), ("zc", 0, 4, 1), ("zb", 1, 3, 1), ("za", 0, 0, 0), ("zd", 1, 0, 1), ("zb", 0, 0, 0),
+    ("bk", 1, 3), ("zd", 1, 4, 0), ("bk", 1, 2), ("za", 0, 0, 1), ("zd", 1, 1, 0), ("zc", 1, 3, 0),
+    ("zc", 1, 3, 1), ("zb", 0, 0, 1), ("bko", 0, 1), ("zd", 0, 2, 0), ("zd", 0, 4, 1), ("zc", 0, 0, 0),
+    ("zd", 1, 4, 1), ("bko", 1, 3), ("zc", 0, 0, 1), ("zd", 0, 3, 0), ("fin", 1, 3), ("fin", 0, 3),
+    ("zd", 1, 3, 0), ("fin", 1, 0), ("zd", 1, 0, 0), ("zd", 0, 1, 1), ("fin", 0, 1), ("zd", 1, 3, 1),
+    ("zd", 0, 2, 1), ("fin", 0, 0), ("bko", 1, 2), ("zd", 0, 0, 0), ("fin", 1, 1), ("zd", 0, 4, 0),
+    ("bko", 0, 2), ("fin", 1, 2), ("fin", 0, 2), ("zd", 0, 0, 1),
 )
 
 
 def kernel(hp, og, w, hg_out, tot_out,
-           ogcat, ogt, whalf, hpc, pbs, pbr, pbo, gs, gr, gown, zs, z1r, z2r, zt,
+           ogcat, ogt, whalf, hpc, pbs, pbr, pbo, gs, gr, gown, zs, z1r, z2r, zt, wide, zgr,
            l_og, l_w, l_hp,
            og_s, og_r, od_s, od_r, w_s, w_r, fn_s, fm_s, f_r, pb_s, pb_r,
-           hp_s, hp_r, g_s, g_r, z1_s, z1_rs, z2_s, z2_rs, z3_s, z3_rs):
+           hp_s, hp_r, g_s, g_r, z1_s, z1_rs, z2_s, z2_rs, z3_s, z3_rs, zg_s, zg_r):
     rows, ff = hp.shape
     depth = w.shape[0]
     half = ff // 2
     fc = half // STEPS
     unit = fc // 2
     part = rows // 2
-    w_rows = depth // WPARTS
+    quarter = depth // 4
+    outer_rows = ((0, 2), (2, 2))
+    inner_rows = ((0, 2), (2, 1), (3, 1))
     piece_rows = depth // PARTS
     fs = lax.axis_index("fs")
     core = lax.axis_index("tp")
@@ -114,9 +122,7 @@
     theirs = [cut(1 - place[q], depth) for q in range(2)]
     far_block = lambda q, p: 2 * (1 - a) + p if q == 0 else 2 * p + 1 - b
     own_block = lambda q, p: 2 * a + p if q == 0 else 2 * p + b
-    low = cut(core, part)
-    mid = pl.ds(pl.multiple_of(rows + core * part, part), part)
-    mid_other = pl.ds(pl.multiple_of(rows + (1 - core) * part, part), part)
+    spans = ((0, part - rows // SHIFT), (part - rows // SHIFT, part + rows // SHIFT))
     both = [(q, p) for q in range(2) for p in range(2)]
     halves = range(PARTS)
 
@@ -146,31 +152,42 @@
     def load_hp(c):
         return pltpu.make_async_copy(hp.at[:, pl.ds(c * fc, fc)], hpc.at[0, c], l_hp.at[c])
 
-    def send_og(q, p):
-        return remote(og.at[low, cut(far_block(q, p), depth)],
-                      ogcat.at[q, mid, cut(p, depth)],
+    def on_core(step):
+        for v in range(2):
+            @pl.when(core == v)
+            def _():
+                step(v)
+
+    def send_og(q, p, v):
+        first, size = spans[v]
+        return remote(og.at[pl.ds(first, size), cut(far_block(q, p), depth)],
+                      ogcat.at[q, pl.ds(rows + first, size), cut(p, depth)],
                       og_s.at[q, p], og_r.at[q, p], token_peer[q])
 
-    def pass_og(q, p, span):
-        spot = ogcat.at[q, span, cut(p, depth)]
+    def pass_og(q, p, v):
+        first, size = spans[v]
+        spot = ogcat.at[q, pl.ds(rows + first, size), cut(p, depth)]
         return remote(spot, spot, od_s.at[q, p], od_r.at[q, p], cpeer)
 
-    def send_w(q, h):
-        c = chunk(q, z)
-        return remote(w.at[h * w_rows:(h + 1) * w_rows, cut(c, fc)],
-                      whalf.at[c, cut(WPARTS * place[q] + h, w_rows)],
-                      w_s.at[q, h], w_r.at[q, h], weight_peer[q])
-
-    def pass_w(q, j, h, peer, ssem):
+    def fetch_w(q, j, part, slot):
+        first, size = part
         c = chunk(q, j)
-        spot = whalf.at[c, cut(WPARTS * (1 - place[q]) + h, w_rows)]
-        return remote(spot, spot, ssem.at[c, h], f_r.at[c, h], peer)
-
-    def near_w(q, j, h):
-        return pass_w(q, j, h, znext, fn_s)
-
-    def mid_w(q, j, h):
-        return pass_w(q, j, h, zmid, fm_s)
+        rows_there = pl.ds(pl.multiple_of(place[q] * depth + first * quarter, quarter), size * quarter)
+        return remote(w.at[pl.ds(first * quarter, size * quarter), cut(c, fc)],
+                      whalf.at[c, rows_there], w_s.at[q, slot], w_r.at[q, slot], weight_peer[q])
+
+    def pass_w(q, j, part, slot, peer, ssem):
+        first, size = part
+        c = chunk(q, j)
+        spot = whalf.at[c, pl.ds(
+            pl.multiple_of((1 - place[q]) * depth + first * quarter, quarter), size * quarter)]
+        return remote(spot, spot, ssem.at[c, slot], f_r.at[c, slot], peer)
+
+    def near_w(q, j, parts, h):
+        return pass_w(q, j, parts[h], h, znext, fn_s)
+
+    def mid_w(q, j, parts, h):
+        return pass_w(q, j, parts[h], h, zmid, fm_s)
 
     def send_hp(q, k):
         j, cols = piece_cols(k)
@@ -188,6 +205,10 @@
     def send_g(q, k, h):
         return remote(strip(gs, q, k, h), strip(gr, q, k, h),
                       g_s.at[q, k, h], g_r.at[q, k, h], weight_peer[q])
+
+    def send_zg(q, h):
+        return remote(strip(gs, q, VIA_Z, h), zgr.at[q, pl.ds(h * piece_rows, piece_rows)],
+                      zg_s.at[q, h], zg_r.at[q, h], znext)
 
     def send_z1(q, k, h):
         return remote(strip(zs, q, k, h), strip(z1r, q, k, h),
@@ -209,9 +230,17 @@
 
     def g_out(q, k, act):
         for h in halves:
-            strip(gs, q, k, h)[...] = jnp.dot(
-                ogt[q, their_rows(q, h), :], act, preferred_element_type=F32).astype(BF)
-            send_g(q, k, h).start()
+            value = jnp.dot(ogt[q, their_rows(q, h), :], act, preferred_element_type=F32)
+            if k == VIA_Z:
+                wide[q, h * piece_rows:(h + 1) * piece_rows] = value
+
+                @pl.when(outer)
+                def _():
+                    strip(gs, q, k, h)[...] = wide[q, h * piece_rows:(h + 1) * piece_rows].astype(BF)
+                    send_zg(q, h).start()
+            else:
+                strip(gs, q, k, h)[...] = value.astype(BF)
+                send_g(q, k, h).start()
 
     def g_own(q, k, act):
         j, cols = piece_cols(k)
@@ -235,12 +264,16 @@
 
     def og_relay(q, far):
         p = og_part(q, far)
-        send_og(q, p).wait_recv()
-        pass_og(q, p, mid).start()
+
+        def step(v):
+            send_og(q, p, v).wait_recv()
+            pass_og(q, p, v).start()
+
+        on_core(step)
 
     def og_whole(q, far):
         p = og_part(q, far)
-        pass_og(q, p, mid_other).wait_recv()
+        on_core(lambda v: pass_og(q, p, 1 - v).wait_recv())
         ogt[q, cut(p, depth), rows:2 * rows] = ogcat[q, rows:2 * rows, cut(p, depth)].T
 
     def grad_send(q, k):
@@ -252,10 +285,19 @@
     def grad_keep(q, k):
         g_own(q, k, act_of(q, k))
 
+    def grad_merge(q, k, h):
+        send_zg(q, h).wait_recv()
+        strip(gs, q, k, h)[...] = (
+            wide[q, h * piece_rows:(h + 1) * piece_rows]
+            + zgr[q, h * piece_rows:(h + 1) * piece_rows].astype(F32)).astype(BF)
+        send_g(q, k, h).start()
+
     def z_outer_send(q, k, h):
-        send_g(q, k, h).wait_recv()
-        strip(zs, q, k, h)[...] = (
-            strip(gown, q, k, h)[...] + strip(gr, q, k, h)[...].astype(F32)).astype(BF)
+        value = strip(gown, q, k, h)[...]
+        if k != VIA_Z:
+            send_g(q, k, h).wait_recv()
+            value = value + strip(gr, q, k, h)[...].astype(F32)
+        strip(zs, q, k, h)[...] = value.astype(BF)
         send_z1(q, k, h).start()
 
     def z_inner_send(q, k, h):
@@ -286,25 +328,42 @@
 
     order = (z, znear, jnp.where(outer, last - znear, last - z), jnp.where(outer, last - z, last - znear))
 
-    def w_own(q, h):
-        send_w(q, h).wait_recv()
-        near_w(q, z, h).start()
+    def w_own(q):
+        fetch_w(q, z, outer_rows[0], 0).wait_recv()
+        near_w(q, z, outer_rows, 0).start()
 
         @pl.when(inner)
         def _():
-            mid_w(q, z, h).start()
+            mid_w(q, z, inner_rows, 0).start()
+
+    def w_own_outer(q):
+        fetch_w(q, z, outer_rows[1], 1).wait_recv()
+        near_w(q, z, outer_rows, 1).start()
+
+    def w_own_inner(q):
+        fetch_w(q, z, inner_rows[1], 1).wait_recv()
+        near_w(q, z, inner_rows, 1).start()
+        mid_w(q, z, inner_rows, 1).start()
+
+    def w_lent(q):
+        fetch_w(q, znear, inner_rows[2], 2).wait_recv()
+        near_w(q, znear, inner_rows, 2).start()
+
+    def w_borrowed(q):
+        near_w(q, z, inner_rows, 2).wait_recv()
+        mid_w(q, z, inner_rows, 2).start()
 
     def w_down(q, h):
-        mid_w(q, last - z, h).wait_recv()
-        near_w(q, last - z, h).start()
+        mid_w(q, last - z, inner_rows, h).wait_recv()
+        near_w(q, last - z, inner_rows, h).start()
 
     def w_across(q, h):
-        near_w(q, znear, h).wait_recv()
-        mid_w(q, znear, h).start()
+        near_w(q, znear, outer_rows, h).wait_recv()
+        mid_w(q, znear, outer_rows, h).start()
 
     def w_far(q, h):
-        mid_w(q, last - znear, h).wait_recv()
-        near_w(q, last - znear, h).start()
+        mid_w(q, last - znear, outer_rows, h).wait_recv()
+        near_w(q, last - znear, outer_rows, h).start()
 
     def back_send(q, i):
         once("w", lambda: [load_w(c) for c in range(2 * STEPS)])
@@ -312,8 +371,9 @@
         if i > 0:
             @pl.when(outer)
             def _():
-                for h in range(WPARTS):
-                    near_w(q, order[i], h).wait_recv()
+                parts = (None, inner_rows[:2], inner_rows, outer_rows)[i]
+                for h in range(len(parts)):
+                    near_w(q, order[i], parts, h).wait_recv()
         pbs[c] = jnp.dot(ogcat[q, rows:2 * rows, :], whalf[c], preferred_element_type=F32).astype(BF)
         send_pb(q, order[i]).start()
 
@@ -328,15 +388,23 @@
         hg_out[:, cut(c, fc)] = (2.0 * positive * (pbo[c] + pbr[c].astype(F32))).astype(BF)
 
     shared = {
-        "sw": lambda q, h: send_w(q, h).start(),
-        "sog": lambda q, far: send_og(q, og_part(q, far)).start(),
+        "sw": lambda q: fetch_w(q, z, outer_rows[0], 0).start(),
+        "sog": lambda q, far: on_core(lambda v: send_og(q, og_part(q, far), v).start()),
         "shp": lambda q, k: send_hp(q, k).start(),
         "tr0": transpose_own, "ogr": og_relay, "ogt": og_whole,
         "gout": grad_send, "gown": grad_keep, "w1": w_own,
         "bk": back_send, "bko": back_keep, "fin": finish,
     }
-    at_outer = {"za": z_outer_send, "zd": z_outer_last}
-    at_inner = {"zb": z_inner_send, "zc": z_inner_last, "w2a": w_down, "w2b": w_across, "w3": w_far}
+    at_outer = {
+        "za": z_outer_send, "zd": z_outer_last, "w1b": w_own_outer, "w1c": w_lent,
+        "sw1": lambda q: fetch_w(q, z, outer_rows[1], 1).start(),
+        "sw2": lambda q: fetch_w(q, znear, inner_rows[2], 2).start(),
+    }
+    at_inner = {
+        "zb": z_inner_send, "zc": z_inner_last, "zg": grad_merge, "w1b": w_own_inner,
+        "w4": w_borrowed, "w2a": w_down, "w2b": w_across, "w3": w_far,
+        "sw1": lambda q: fetch_w(q, z, inner_rows[1], 1).start(),
+    }
 
     def run_group(table, role, group):
         steps = [(table[name], args) for name, *args in group if name in table]
@@ -376,34 +444,49 @@
     run_group(at_outer, outer, group)
     run_group(at_inner, inner, group)
 
-    for q, p in both:
-        send_og(q, p).wait_send()
-        pass_og(q, p, mid).wait_send()
+    def og_sent(v):
+        for q, p in both:
+            send_og(q, p, v).wait_send()
+            pass_og(q, p, v).wait_send()
+
+    on_core(og_sent)
     for q in range(2):
-        for h in range(WPARTS):
-            send_w(q, h).wait_send()
-            near_w(q, z, h).wait_send()
+        fetch_w(q, z, outer_rows[0], 0).wait_send()
+        near_w(q, z, outer_rows, 0).wait_send()
         for k in range(count):
             send_hp(q, k).wait_send()
         for j in range(STEPS):
             send_pb(q, j).wait_send()
     pieces = [(q, k, h) for k in range(count) for q in range(2) for h in halves]
     for q, k, h in pieces:
-        send_g(q, k, h).wait_send()
+        if k != VIA_Z:
+            send_g(q, k, h).wait_send()
 
     @pl.when(outer)
     def _():
+        for q in range(2):
+            fetch_w(q, z, outer_rows[1], 1).wait_send()
+            fetch_w(q, znear, inner_rows[2], 2).wait_send()
+            near_w(q, z, outer_rows, 1).wait_send()
+            near_w(q, znear, inner_rows, 2).wait_send()
+            for h in halves:
+                send_zg(q, h).wait_send()
         for q, k, h in pieces:
             send_z1(q, k, h).wait_send()
 
     @pl.when(inner)
     def _():
         for q in range(2):
-            for h in range(WPARTS):
-                mid_w(q, z, h).wait_send()
-                mid_w(q, znear, h).wait_send()
-                near_w(q, last - z, h).wait_send()
-                near_w(q, last - znear, h).wait_send()
+            fetch_w(q, z, inner_rows[1], 1).wait_send()
+            near_w(q, z, inner_rows, 1).wait_send()
+            for h in range(3):
+                mid_w(q, z, inner_rows, h).wait_send()
+                near_w(q, last - z, inner_rows, h).wait_send()
+            for h in range(2):
+                mid_w(q, znear, outer_rows, h).wait_send()
+                near_w(q, last - znear, outer_rows, h).wait_send()
+            for h in halves:
+                send_g(q, VIA_Z, h).wait_send()
         for q, k, h in pieces:
             send_z2(q, k, h).wait_send()
             send_z3(q, k, h).wait_send()
@@ -430,6 +513,7 @@
     chunks = 2 * STEPS
     fc = ff // chunks
     count = len(PIECES)
+    via = PIECES[VIA_Z][2] * fc // 2
     any_spec = pl.BlockSpec(memory_space=pl.ANY)
     vmem_spec = pl.BlockSpec(memory_space=pltpu.VMEM)
 
@@ -450,9 +534,10 @@
             block(rows, BF), block(rows, BF), block(rows, F32),
             block(depth, BF), block(depth, BF), block(depth, F32),
             block(depth, BF), block(depth, BF), block(depth, BF), block(depth, BF),
+            pltpu.VMEM((2, depth, via), F32), pltpu.VMEM((2, depth, via), BF),
             sem((2, 2)), sem((chunks,)), sem((chunks,)),
-        ] + [sem((2, 2))] * 4 + [sem((2, WPARTS))] * 2 + [sem((chunks, WPARTS))] * 3 + [sem((chunks,))] * 2
-        + [sem((2, count))] * 2 + [sem((2, count, PARTS))] * 8,
+        ] + [sem((2, 2))] * 4 + [sem((2, 3))] * 2 + [sem((chunks, 3))] * 3 + [sem((chunks,))] * 2
+        + [sem((2, count))] * 2 + [sem((2, count, PARTS))] * 8 + [sem((2, PARTS))] * 2,
         compiler_params=pltpu.CompilerParams(
             collective_id=0, has_side_effects=True, vmem_limit_bytes=48 * 1024 * 1024
         ),

time: 96.1 us -> 95.5 us (level)
  no operation moved by 1% of the time
where the time goes in v5:
time: 95.5 us; the launch traced here: 95.3 us
  Pallas kernels  94.5 us (99%)
    pallas_call x1, Pallas kernels, paired_body(): pl.pallas_call(kernel, out_shape=(jax.ShapeDtypeStruct((rows, ff), BF), j...  91.8 us
    pallas_call x1, Pallas kernels, paired_body(): pl.pallas_call(put_kernel, out_shape=(jax.ShapeDtypeStruct((rows, ff), BF...  2.74 us

profile of v5, /device:TPU:0, one launch (start us, length us, event | category | flops | bytes accessed | tf_op | source)
XLA Modules:
  0.0 95.3 jit_solution(17795701433865450361)
XLA Ops:
  0.6 91.8 %shard_map.50 = (bf16[512,2048]{1,0:T(8,128)(2,1)S(1)}, bf16[512,2048]{1,0:T(8,128)(2,1)S(1)}) custom-call(bf16[512,2048]{1,0:T(8,128)(2,1)} %hp.1, bf16[512,2048]{1,0:T(8,128)(2,1)} %og.1, bf16[512,2048]{1,0:T(8,128)(2,1)} %w.1), custom_call_target="tpu_custom_call" | custom-call | tf_op jit(solution)/shard_map/pallas_call | solution.py:524
  92.4 2.7 %shard_map.51 = (bf16[512,2048]{1,0:T(8,128)(2,1)}, f32[512,2048]{1,0:T(8,128)}) custom-call(bf16[512,2048]{1,0:T(8,128)(2,1)S(1)} %get-tuple-element.4.hg, bf16[512,2048]{1,0:T(8,128)(2,1)S(1)} %get-tuple-element.5.total), custom_call_target="tpu_custom_call" | custom-call | tf_op jit(solution)/shard_map/pallas_call | solution.py:545
